TPU v7x, 512 devices: a whole 4x4x16 slice. The times are simulated.
512 devices in a mesh: sp: 32 (over z, core), tp: 16 (over y, x).
Axes of the slice: x: 4, y: 4, z: 16, core: 2. Of those that a mesh axis runs over, the one named last changes fastest.
Arguments:
- query_rows: bfloat16 [16384, 1024], P('sp', 'tp'), may hold values from -128 to 128
- key_rows: bfloat16 [16384, 1024], P('sp', 'tp'), may hold values from -4 to 4
- value_rows: bfloat16 [16384, 1024], P('sp', 'tp'), may hold values from -6 to 6
- cum_gates: float32 [16384, 16], P('sp', 'tp'), may hold values from -16386 to 0, as said below
- residual: bfloat16 [16384, 2048], P('sp', 'tp'), may hold values from -64 to 64
- output_weight: bfloat16 [1024, 2048], P(None, 'tp'), may hold values from -0.1875 to 0.1875
- norm_gain: bfloat16 [2048], replicated, may hold values from 0.099609375 to 1.8984375
- expert_index: int32 [16384, 2], P('sp'), may hold values from 0 to 31, all different within a row; in each aligned block of 512 rows (0 to 511, 512 to 1023, ...) at most 64 rows name the same one
- route_weights: float32 [16384, 2], P('sp'), may hold values from 0.2 to 1
- gate_weight: bfloat16 [32, 2048, 2048], P('sp', None, 'tp'), may hold values from -2 to 2
- up_weight: bfloat16 [32, 2048, 2048], P('sp', None, 'tp'), may hold values from -2 to 2
- down_weight: bfloat16 [32, 2048, 2048], P('sp', None, 'tp'), may hold values from -0.125 to 0.125
Outputs:
- layer_out: bfloat16 [16384, 2048], P('sp', 'tp')
Inputs may be any that keep to these rules, and one draw needn't show every extreme that they name: `cum_gates`: each head's values never rise along positions. `expert_index`: each token names 2 different experts. In the 512 tokens of one index of sp no expert is named more than 64 times, and in some index's tokens some expert is named exactly 64 times.
All inputs are finite; a program needn't handle non-finite values.
Results may differ from a plain program's by a relative error of at most 0.01.
Values may be sent and summed in bfloat16 or wider, within the bound.
A program may use at most 64 MiB of HBM per device.

v0:
```python
import math

import jax
import jax.numpy as jnp
from jax import lax
from jax.sharding import PartitionSpec as P

NORM_EPS = 1e-06
CLAMP_LIMIT = 7.0
SILU_ALPHA = 1.702


def joined_along(parts, dim):
    lengths = list(parts.shape[1:])
    lengths[dim] *= parts.shape[0]
    return jnp.moveaxis(parts, 0, dim).reshape(lengths)


def copy_for_each(x, axis):
    copies = jnp.broadcast_to(x, (lax.axis_size(axis), *x.shape))
    return lax.all_to_all(copies, axis, split_axis=0, concat_axis=0, tiled=True)


def gathered_copies(x, axis, dim):
    return joined_along(copy_for_each(x, axis), dim)


def side_by_side(arrays, axis, dim, along):
    widths = [a.shape[along] for a in arrays]
    both = jnp.concatenate(arrays, axis=along)
    result = lax.all_gather(both, axis, axis=dim, tiled=True)
    return tuple(jnp.split(result, [sum(widths[:k]) for k in range(1, len(widths))], axis=along))


def normalize(rows, norm_gain):
    wide = rows.astype(jnp.float32)
    factor = lax.rsqrt(jnp.mean(wide * wide, axis=-1, keepdims=True) + NORM_EPS)
    return (wide * factor * norm_gain.astype(jnp.float32)).astype(jnp.bfloat16)


def attend_local(query_rows, key_rows, value_rows, cum_gates):
    rows = query_rows.shape[0]
    heads_here = cum_gates.shape[1]
    head_size = query_rows.shape[1] // heads_here
    first_place = lax.axis_index("sp") * rows
    all_gates = gathered_copies(cum_gates, "sp", 0)
    queries = query_rows.reshape(rows, heads_here, head_size)
    query_place = first_place + jnp.arange(rows, dtype=jnp.int32)
    root_scale = head_size ** (-0.5)
    start_state = (
        jnp.full((rows, heads_here), -jnp.inf, jnp.float32),
        jnp.zeros((rows, heads_here), jnp.float32),
        jnp.zeros((rows, heads_here, head_size), jnp.float32),
    )
    key_piece, value_piece = side_by_side((key_rows, value_rows), "sp", 0, 1)
    count = key_piece.shape[0]
    block = math.gcd(count, 512)

    def one_block(number, state):
        top, total, summed = state
        offset = number * block
        key_block = lax.dynamic_slice_in_dim(key_piece, number * block, block, 0).reshape(
            block, heads_here, head_size
        )
        value_block = lax.dynamic_slice_in_dim(value_piece, number * block, block, 0).reshape(
            block, heads_here, head_size
        )
        gate_block = lax.dynamic_slice_in_dim(all_gates, offset, block, 0)
        scores = (
            jnp.einsum("qhd,khd->qhk", queries, key_block, preferred_element_type=jnp.float32)
            * root_scale
        )
        scores = scores + cum_gates[:, :, None] - gate_block.T[None, :, :]
        key_place = offset + jnp.arange(block, dtype=jnp.int32)
        allowed = key_place[None, :] <= query_place[:, None]
        scores = jnp.where(allowed[:, None, :], scores, -jnp.inf)
        new_top = jnp.maximum(top, jnp.max(scores, axis=-1))
        safe_top = jnp.where(new_top == -jnp.inf, 0.0, new_top)
        raised = jnp.exp(scores - safe_top[:, :, None])
        shrink = jnp.exp(top - safe_top)
        total = total * shrink + jnp.sum(raised, axis=-1)
        summed = summed * shrink[:, :, None] + jnp.einsum(
            "qhk,khd->qhd",
            raised.astype(jnp.bfloat16),
            value_block,
            preferred_element_type=jnp.float32,
        )
        return (new_top, total, summed)

    def compute(state):
        return lax.fori_loop(0, count // block, one_block, state)

    def keep_state(state):
        return state

    top, total, summed = lax.cond(
        jnp.int32(0) <= first_place + rows - 1, compute, keep_state, start_state
    )
    return (summed / total[:, :, None]).astype(jnp.bfloat16).reshape(rows, heads_here * head_size)


def body(
    query_rows,
    key_rows,
    value_rows,
    cum_gates,
    residual,
    output_weight,
    norm_gain,
    expert_index,
    route_weights,
    gate_weight,
    up_weight,
    down_weight,
):
    attended = attend_local(query_rows, key_rows, value_rows, cum_gates)
    weight_rows = output_weight
    projected = jnp.dot(
        gathered_copies(attended, "tp", 1), weight_rows, preferred_element_type=jnp.float32
    )
    mixed = (residual.astype(jnp.float32) + projected).astype(jnp.bfloat16)
    rows = residual.shape[0]
    topk = expert_index.shape[1]
    local_experts = gate_weight.shape[0]
    groups = lax.axis_size("sp")
    experts = local_experts * groups
    capacity = 2 * rows * topk // experts
    chosen = expert_index.reshape(rows * topk)
    matches = (chosen[:, None] == jnp.arange(experts, dtype=jnp.int32)[None, :]).astype(jnp.int32)
    rank = jnp.sum((jnp.cumsum(matches, axis=0) - matches) * matches, axis=1)
    slot = chosen * capacity + rank
    owner = jnp.arange(rows * topk, dtype=jnp.int32) // topk
    slot_token = jnp.full((experts * capacity,), rows, jnp.int32).at[slot].set(owner)
    padded = jnp.concatenate([mixed, jnp.zeros((1, mixed.shape[1]), mixed.dtype)], axis=0)
    outgoing = padded[slot_token].reshape(experts, capacity, mixed.shape[1])
    arrived = lax.all_to_all(outgoing, "sp", split_axis=0, concat_axis=0, tiled=True)
    count = arrived.shape[1]
    grouped = arrived.reshape(groups, local_experts, count, arrived.shape[2])
    normed = normalize(lax.all_gather(grouped, "tp", axis=3, tiled=True), norm_gain)
    gate_input = jnp.einsum(
        "seid,edf->seif", normed, gate_weight, preferred_element_type=jnp.float32
    )
    linear_input = jnp.einsum(
        "seid,edf->seif", normed, up_weight, preferred_element_type=jnp.float32
    )
    gate_cut = jnp.minimum(gate_input, CLAMP_LIMIT)
    linear_cut = jnp.clip(linear_input, -CLAMP_LIMIT, CLAMP_LIMIT)
    activated = (gate_cut * jax.nn.sigmoid(SILU_ALPHA * gate_cut) * (linear_cut + 1.0)).astype(
        jnp.bfloat16
    )
    weight_rows = down_weight
    produced = jnp.einsum(
        "seif,efc->seic",
        lax.all_gather(activated, "tp", axis=3, tiled=True),
        weight_rows,
        preferred_element_type=jnp.float32,
    ).astype(jnp.bfloat16)
    returned = lax.all_to_all(
        produced.reshape(groups * local_experts, count, down_weight.shape[2]),
        "sp",
        split_axis=0,
        concat_axis=0,
        tiled=True,
    )
    flat = returned.reshape(experts * capacity, returned.shape[2])
    picked = flat[slot].reshape(rows, topk, flat.shape[1]).astype(jnp.float32)
    blended = jnp.sum(route_weights[:, :, None] * picked, axis=1)
    return (mixed.astype(jnp.float32) + blended).astype(jnp.bfloat16)


def solution(mesh):
    placed = (
        P("sp", "tp"),
        P("sp", "tp"),
        P("sp", "tp"),
        P("sp", "tp"),
        P("sp", "tp"),
        P(None, "tp"),
        P(),
        P("sp", None),
        P("sp", None),
        P("sp", None, "tp"),
        P("sp", None, "tp"),
        P("sp", None, "tp"),
    )
    return jax.shard_map(body, mesh=mesh, in_specs=placed, out_specs=P("sp", "tp"), check_vma=False)
```

profile of v0, /device:TPU:25, one launch (start us, length us, event | category | flops | bytes accessed | tf_op | source)
XLA Modules:
  0.0 566.8 jit_solution(3906957129772426121)
XLA Ops:
  10.7 15.9 %all-to-all-start = ((f32[32,512,1]{1,2,0:T(1,128)}), f32[32,512,1]{1,2,0:T(1,128)S(1)}, u32[]{:S(2)}, u32[]{:S(2)}) async-start(f32[32,512,1]{1,2,0:T(1,128)} %broadcast_in_dim.66), calls=%async_computation | async-start | bytes 131072 | tf_op jit(solution)/shard_map/all_to_all | solution.py:21
  27.6 12.0 %all-to-all-done = f32[32,512,1]{1,2,0:T(1,128)S(1)} async-done(((f32[32,512,1]{1,2,0:T(1,128)}), f32[32,512,1]{1,2,0:T(1,128)S(1)}, u32[]{:S(2)}, u32[]{:S(2)}) %all-to-all-start) | async-done | bytes 65568 | tf_op jit(solution)/shard_map/all_to_all | solution.py:21
  39.6 48.4 %all-gather.5.cloned.1.call-done = bf16[16384,128]{1,0:T(8,128)(2,1)} async-done(((bf16[512,128]{1,0:T(8,128)(2,1)}), bf16[16384,128]{1,0:T(8,128)(2,1)}) %all-gather.5.cloned.1.call-update) | async-done | bytes 4194320 | tf_op jit(solution)/shard_map/all_gather | solution.py:31
  88.0 153.2 %conditional.1 = (f32[512,1]{0,1:T(1,128)}, f32[512,1,64]{0,2,1:T(8,128)}) conditional(s32[]{:T(128)} %convert_element_type.57, () %tuple.27, (bf16[16384,128]{1,0:T(8,128)(2,1)}, f32[32,512,1]{1,2,0:T(1,128)S(1)}, bf16[512,64]{0,1:T(8,128)(2,1)}, s32[]{:T(128)}, s32[512]{0:T(512)S(1)}, /*index=5*/f32[512,1]{0,1:T(1,128)}) %tuple.28), branch_computations={%region_0.0_spmd, %region_1.6_spmd} | conditional | flops 69834240 | bytes 12448155 | solution.py:96
  88.1 7.3 %fusion.71 = (bf16[16384,64]{1,0:T(8,128)(2,1)}, bf16[16384,64]{1,0:T(8,128)(2,1)}) fusion(bf16[16384,128]{1,0:T(8,128)(2,1)} %get-tuple-element.194), kind=kLoop, calls=%fused_computation.85 | loop fusion | bytes 8388608 | tf_op jit(solution)/shard_map/split | solution.py:32
  95.4 145.9 %while.17 = (s32[]{:T(128)}, f32[512,1]{0,1:T(1,128)S(1)}, f32[512,1]{0,1:T(1,128)}, f32[512,1,64]{0,2,1:T(8,128)}, s32[512]{0:T(512)S(1)}, /*index=5*/bf16[1638...) while((s32[]{:T(128)}, f32[512,1]{0,1:T(1,128)S(1)}, ...), condition=%wide.region_5.5_spmd.clone, body=%wide.region_2.4_spmd.clone.sunk | while | flops 69833728 | bytes 3784919 | solution.py:91
  102.0 1.9 fusion.85
  106.6 1.9 fusion.85
  111.2 1.9 fusion.85
  115.7 1.9 fusion.85
  120.3 1.9 fusion.85
  124.9 1.9 fusion.85
  129.5 1.9 fusion.85
  138.6 1.9 fusion.85
  143.2 1.9 fusion.85
  147.8 1.9 fusion.85
  157.0 1.9 fusion.85
  161.5 1.9 fusion.85
  166.1 1.9 fusion.85
  170.7 1.9 fusion.85
  175.3 1.9 fusion.85
  179.8 1.9 fusion.85
  184.4 1.9 fusion.85
  193.6 1.9 fusion.85
  198.2 1.9 fusion.85
  202.7 1.9 fusion.85
  207.3 1.9 fusion.85
  211.9 1.9 fusion.85
  216.5 1.9 fusion.85
  221.1 1.9 fusion.85
  230.2 1.9 fusion.85
  234.8 1.9 fusion.85
  239.4 1.9 fusion.85
  243.3 6.6 %all-to-all-start.1 = ((bf16[16,512,64]{1,2,0:T(8,128)(2,1)}), bf16[16,512,64]{1,2,0:T(8,128)(2,1)S(1)}, u32[]{:S(2)}, u32[]{:S(2)}) async-start(bf16[16,512,64]{1,2,0:T(8,128)(2,1)} %broadcast_in_dim.67), calls=%async_computation.1 | async-start | bytes 2097152 | tf_op jit(solution)/shard_map/all_to_all | solution.py:21
  250.5 9.0 %reduce-window.6 = s32[32,8,128]{2,1,0:T(8,128)S(1)} reduce-window(s32[32,8,128]{2,1,0:T(8,128)S(1)} %fusion.61, s32[]{:T(128)} %constant.103.clone.1), window={size=1x1x128 pad=0_0x0_0x127_0}, to_apply=%region_6.7 | reduce-window | flops 4161536 | bytes 262148 | tf_op jit(solution)/shard_map/reduce-window
  260.1 4.3 scatter_custom_fusion
  264.9 6.2 %gather_fusion = bf16[2048,128]{1,0:T(8,128)(2,1)S(1)} fusion(bf16[513,128]{1,0:T(8,128)(2,1)S(1)} %concatenate.7, s32[2048]{0:T(1024)S(1)} %fusion.63), kind=kCustom, calls=%fused_computation | custom fusion | bytes 1056768 | tf_op jit(solution)/shard_map/gather | solution.py:135
  271.1 42.4 %all_to_all.20 = bf16[32,64,128]{2,1,0:T(8,128)(2,1)} all-to-all(bf16[32,64,128]{2,1,0:T(8,128)(2,1)S(1)} %bitcast.160), channel_id=1, replica_groups=mesh['sp'=32,'tp'=16] {'sp'}, dimensions={0} | all-to-all | bytes 1048576 | tf_op jit(solution)/shard_map/all_to_all | solution.py:136
  313.8 81.0 %all-gather.9.cloned.1.call-done = bf16[32,64,2048]{2,1,0:T(8,128)(2,1)} async-done(((bf16[32,64,128]{2,1,0:T(8,128)(2,1)}), bf16[32,64,2048]{2,1,0:T(8,128)(2,1)}) %all-gather.9.cloned.1.call-update) | async-done | bytes 8388624 | tf_op jit(solution)/shard_map/all_gather | solution.py:139
  394.8 5.2 fusion.19
  400.6 2.7 fusion.32
  403.3 3.7 fusion.47
  407.0 92.1 %all-gather.7.cloned.1.call-done = bf16[32,1,64,2048]{3,2,0,1:T(8,128)(2,1)} async-done(((bf16[32,1,64,128]{3,2,0,1:T(8,128)(2,1)}), bf16[32,1,64,2048]{3,2,0,1:T(8,128)(2,1)}) %all-gather.7.cloned.1.call-update) | async-done | bytes 8388624 | tf_op jit(solution)/shard_map/all_gather | solution.py:154
  499.2 6.6 %fusion.50 = bf16[32,64,128]{2,1,0:T(8,128)(2,1)} fusion(bf16[32,1,64,2048]{3,2,0,1:T(8,128)(2,1)} %all-gather.7.cloned.1.call-done, bf16[1,2048,128]{2,1,0:T(8,128)(2,1)S(1)} %copy-done.9), kind=kOutput, calls=%fused_computation.49 | convolution fusion | flops 1074003968 | bytes 9437184 | tf_op jit(solution)/shard_map/seif,efc->seic/dot_general | solution.py:152
  505.7 14.4 %all-to-all-start.3 = ((bf16[32,64,128]{2,1,0:T(8,128)(2,1)}), bf16[32,64,128]{2,1,0:T(8,128)(2,1)S(1)}, u32[]{:S(2)}, u32[]{:S(2)}) async-start(bf16[32,64,128]{2,1,0:T(8,128)(2,1)} %fusion.50), calls=%async_computation.3 | async-start | bytes 1048576 | tf_op jit(solution)/shard_map/all_to_all | solution.py:158
  520.3 33.3 %all-to-all-done.3 = bf16[32,64,128]{2,1,0:T(8,128)(2,1)S(1)} async-done(((bf16[32,64,128]{2,1,0:T(8,128)(2,1)}), bf16[32,64,128]{2,1,0:T(8,128)(2,1)S(1)}, u32[]{:S(2)}, u32[]{:S(2)}) %all-to-all-start.3) | async-done | bytes 524320 | tf_op jit(solution)/shard_map/all_to_all | solution.py:158
  553.6 3.2 gather_fusion.1
  556.8 2.8 fusion.54
  (293 shorter events, 103.7 us)
Async XLA Ops:
  6.5 393.5 %copy-start = (bf16[1,2048,128]{2,1,0:T(8,128)(2,1)S(1)}, bf16[1,2048,128]{2,1,0:T(8,128)(2,1)}, u32[]{:S(2)}) copy-start(bf16[1,2048,128]{2,1,0:T(8,128)(2,1)} %param.25) | copy-start | bytes 1572868
  6.5 81.5 %all-gather.5.cloned.1.call-start = ((), (), s32[]{:S(2)}) async-start(), calls=%async_computation.4 | async-start | bytes 4325376 | tf_op jit(solution)/shard_map/all_gather | solution.py:31
  10.7 28.9 %all-to-all-start = ((f32[32,512,1]{1,2,0:T(1,128)}), f32[32,512,1]{1,2,0:T(1,128)S(1)}, u32[]{:S(2)}, u32[]{:S(2)}) async-start(f32[32,512,1]{1,2,0:T(1,128)} %broadcast_in_dim.66), calls=%async_computation | async-start | bytes 131072 | tf_op jit(solution)/shard_map/all_to_all | solution.py:21
  88.0 162.0 %copy-start.4 = (s32[512,2]{0,1:T(2,128)S(1)}, s32[512,2]{0,1:T(2,128)}, u32[]{:S(2)}) copy-start(s32[512,2]{0,1:T(2,128)} %param.23) | copy-start | bytes 12292
  88.0 176.4 %copy-start.2 = (bf16[1024,128]{1,0:T(8,128)(2,1)S(1)}, bf16[1024,128]{1,0:T(8,128)(2,1)}, u32[]{:S(2)}) copy-start(bf16[1024,128]{1,0:T(8,128)(2,1)} %param.21) | copy-start | bytes 786436
  88.0 176.4 %copy-start.3 = (bf16[512,128]{1,0:T(8,128)(2,1)S(1)}, bf16[512,128]{1,0:T(8,128)(2,1)}, u32[]{:S(2)}) copy-start(bf16[512,128]{1,0:T(8,128)(2,1)} %param.20) | copy-start | bytes 393220
  88.1 7.3 %copy-start.7 = (f32[512,1]{0,1:T(1,128)S(1)}, f32[512,1]{0,1:T(1,128)}, u32[]{:S(2)}) copy-start(f32[512,1]{0,1:T(1,128)} %get-tuple-element.359) | copy-start | bytes 6148 | tf_op jit(solution)/shard_map/cond
  88.1 7.3 %copy-start.10 = (bf16[512,64]{0,1:T(8,128)(2,1)S(1)}, bf16[512,64]{0,1:T(8,128)(2,1)}, u32[]{:S(2)}) copy-start(bf16[512,64]{0,1:T(8,128)(2,1)} %get-tuple-element.205) | copy-start | bytes 196612 | tf_op jit(solution)/shard_map/cond
  241.3 72.5 %copy-start.6 = (bf16[2048]{0:T(1024)(128)(2,1)S(1)}, bf16[2048]{0:T(1024)(128)(2,1)}, u32[]{:S(2)}) copy-start(bf16[2048]{0:T(1024)(128)(2,1)} %param.22) | copy-start | bytes 12292
  243.3 21.1 %all-to-all-start.1 = ((bf16[16,512,64]{1,2,0:T(8,128)(2,1)}), bf16[16,512,64]{1,2,0:T(8,128)(2,1)S(1)}, u32[]{:S(2)}, u32[]{:S(2)}) async-start(bf16[16,512,64]{1,2,0:T(8,128)(2,1)} %broadcast_in_dim.67), calls=%async_computation.1 | async-start | bytes 2097152 | tf_op jit(solution)/shard_map/all_to_all | solution.py:21
  250.0 144.8 %all-gather.9.cloned.1.call-start = ((), (), s32[]{:S(2)}) async-start(), calls=%async_computation.6 | async-start | bytes 8912896 | tf_op jit(solution)/shard_map/all_gather | solution.py:139
  313.5 185.6 %all-gather.7.cloned.1.call-start = ((), (), s32[]{:S(2)}) async-start(), calls=%async_computation.5 | async-start | bytes 8912896 | tf_op jit(solution)/shard_map/all_gather | solution.py:154
  394.8 5.8 %copy-start.1 = (bf16[32,64,2048]{2,1,0:T(8,128)(2,1)S(1)}, bf16[32,64,2048]{2,1,0:T(8,128)(2,1)}, u32[]{:S(2)}) copy-start(bf16[32,64,2048]{2,1,0:T(8,128)(2,1)} %all-gather.9.cloned.1.call-done) | copy-start | bytes 25165828
  400.6 2.7 copy-start.8
  403.3 95.9 %copy-start.9 = (bf16[1,2048,128]{2,1,0:T(8,128)(2,1)S(1)}, bf16[1,2048,128]{2,1,0:T(8,128)(2,1)}, u32[]{:S(2)}) copy-start(bf16[1,2048,128]{2,1,0:T(8,128)(2,1)} %param.27) | copy-start | bytes 1572868
  407.0 113.1 %copy-start.5 = (f32[512,2]{0,1:T(2,128)S(1)}, f32[512,2]{0,1:T(2,128)}, u32[]{:S(2)}) copy-start(f32[512,2]{0,1:T(2,128)} %param.24) | copy-start | bytes 12292
  505.7 47.9 %all-to-all-start.3 = ((bf16[32,64,128]{2,1,0:T(8,128)(2,1)}), bf16[32,64,128]{2,1,0:T(8,128)(2,1)S(1)}, u32[]{:S(2)}, u32[]{:S(2)}) async-start(bf16[32,64,128]{2,1,0:T(8,128)(2,1)} %fusion.50), calls=%async_computation.3 | async-start | bytes 1048576 | tf_op jit(solution)/shard_map/all_to_all | solution.py:158
Sparse Core Ops, SparseCore 0:
  9.5 78.5 all-gather.4
  313.7 81.1 all-gather.8
  407.1 91.9 all-gather.6
where the time goes:
time: 571 us; the launch traced here: 567 us
  waiting for transfers between devices  267 us (47%)
  matrix products  115 us (20%)
  other arithmetic  63 us (11%)
  blocking collectives  42.4 us (7%)
  starting transfers between devices  37.2 us (7%)
  local copies, waits for them, and re-layouts  28 us (5%)
  between operations  13.4 us (2%)
    all_gather x1, waiting for transfers between devices, body(): lax.all_gather(activated, 'tp', axis=3, tiled=True)  92.1 us
    all_gather x1, waiting for transfers between devices, body(): lax.all_gather(grouped, 'tp', axis=3, tiled=True)  81 us
    dot_general x32, matrix products, one_block(): jnp.einsum('qhk,khd->qhd', raised.astype(jnp.bfloat16), value_block, pref...  61.4 us
    all_gather x1, waiting for transfers between devices, side_by_side(): result = lax.all_gather(both, axis, axis=dim, tiled=True)  48.4 us
    all_to_all x1, blocking collectives, body(): lax.all_to_all(outgoing, 'sp', split_axis=0, concat_axis=0, tiled=True)  42.4 us
    dot_general x32, matrix products, one_block(): jnp.einsum('qhd,khd->qhk', queries, key_block, preferred_element_type=jnp...  40.4 us
    add x32, other arithmetic, one_block(): total = total * shrink + jnp.sum(raised, axis=-1)  36.7 us
    all_to_all x1, waiting for transfers between devices, body(): lax.all_to_all(produced.reshape(groups * local_experts, count, down_weigh...  33.3 us
  transfers between devices with their start and end apart: 6, of which 5 were waited for; matrix products, arithmetic and copies ran while one was open for 3% of the time, Pallas kernels for 0%

commit v1 on v0

v1 whole, which is shorter than its diff:
```python
import functools
import math

import jax
import jax.numpy as jnp
from jax import lax
from jax.experimental import pallas as pl
from jax.experimental.pallas import tpu as pltpu
from jax.sharding import PartitionSpec as P

NORM_EPS = 1e-06
CLAMP_LIMIT = 7.0
SILU_ALPHA = 1.702
MESH = pl.DeviceIdType.MESH
GATE_ROWS = 16


def remote(src, dst, send_sem, recv_sem, **where):
    return pltpu.make_async_remote_copy(
        src_ref=src,
        dst_ref=dst,
        send_sem=send_sem,
        recv_sem=recv_sem,
        device_id=where,
        device_id_type=MESH,
    )


def attention_kernel(
    sp_size,
    tp_size,
    q_ref,
    k_ref,
    v_ref,
    gate_ref,
    residual_ref,
    weight_ref,
    mixed_ref,
    kv_all,
    qpad,
    wide,
    top,
    total,
    summed,
    att_all,
    kv_recv,
    own_recv,
    ring_send,
    pair_send,
    att_recv,
    att_send,
):
    chips = sp_size // 2
    ups = chips // 2
    downs = chips - 1 - ups
    sp = lax.axis_index("sp")
    tp = lax.axis_index("tp")
    chip = sp // 2
    core = sp - 2 * chip
    rows, size = q_ref.shape
    half = rows // 2
    cut = (GATE_ROWS + rows) // 2
    up_sp = lax.rem(chip + 1, chips) * 2 + core
    down_sp = lax.rem(chip + chips - 1, chips) * 2 + core
    pair_sp = chip * 2 + 1 - core

    barrier = pltpu.get_barrier_semaphore()
    for target in (up_sp, down_sp, pair_sp):
        pl.semaphore_signal(barrier, inc=1, device_id={"sp": target}, device_id_type=MESH)
    for d in range(1, tp_size):
        pl.semaphore_signal(
            barrier, inc=1, device_id={"tp": lax.rem(tp + d, tp_size)}, device_id_type=MESH
        )

    gates = gate_ref[...]
    high = gates.astype(jnp.bfloat16)
    rest = gates - high.astype(jnp.float32)
    middle = rest.astype(jnp.bfloat16)
    low = (rest - middle.astype(jnp.float32)).astype(jnp.bfloat16)
    kv_all[sp, 0:GATE_ROWS, :] = jnp.concatenate(
        [
            high.astype(jnp.float32),
            middle.astype(jnp.float32),
            low.astype(jnp.float32),
            jnp.zeros_like(gates),
        ],
        axis=0,
    ).astype(jnp.bfloat16)
    kv_all[sp, GATE_ROWS:, :] = jnp.concatenate([k_ref[...], v_ref[...]], axis=1)
    qs = (q_ref[...].astype(jnp.float32) * (size**-0.5)).astype(jnp.bfloat16)
    qpad[...] = jnp.concatenate([qs, jnp.zeros_like(qs)], axis=1)
    first_gate = gates[0:1, 0:1]

    pl.semaphore_wait(barrier, 3 + tp_size - 1)

    def piece(slot, part):
        return kv_all.at[slot, pl.ds(part * cut, cut), :]

    def hop(slot, step, way, part, target):
        return remote(
            piece(slot, part),
            piece(slot, part),
            ring_send.at[step, way, part],
            kv_recv.at[slot, part],
            sp=target,
        )

    def share(slot, step, way):
        return remote(
            kv_all.at[slot],
            kv_all.at[slot],
            pair_send.at[step, way],
            own_recv.at[slot],
            sp=pair_sp,
        )

    if ups >= 1:
        for part in range(2):
            hop(sp, 0, 0, part, up_sp).start()
            if downs >= 1:
                hop(sp, 0, 1, part, down_sp).start()
    share(sp, 0, 0).start()

    wide[...] = jnp.zeros_like(wide)
    for h in range(tp_size):
        w = weight_ref[h * size : (h + 1) * size, :]
        wide[h * 2 * size : h * 2 * size + size, 0 : w.shape[1]] = w
        wide[h * 2 * size + size : (h + 1) * 2 * size, w.shape[1] :] = w

    top[...] = jnp.full_like(top, -1e30)
    total[...] = jnp.zeros_like(total)
    summed[...] = jnp.zeros_like(summed)
    tile = min(128, rows)
    lanes = 128

    def attend(slot, diagonal):
        parts = kv_all[slot, 0:GATE_ROWS, :].astype(jnp.float32)
        n4 = GATE_ROWS // 4
        key_gates = parts[0:n4] + parts[n4 : 2 * n4] + parts[2 * n4 : 3 * n4]
        shift = first_gate - key_gates
        keys = kv_all[slot, GATE_ROWS:, :]
        for t in range(rows // tile):
            here = slice(t * tile, (t + 1) * tile)
            scores = lax.dot_general(
                qpad[here, :], keys, (((1,), (1,)), ((), ())), preferred_element_type=jnp.float32
            )
            pieces = []
            for j in range(rows // lanes):
                s = scores[:, j * lanes : (j + 1) * lanes] + shift[j : j + 1, :]
                if diagonal:
                    place = lax.broadcasted_iota(jnp.int32, s.shape, 0) + t * tile
                    other = lax.broadcasted_iota(jnp.int32, s.shape, 1) + j * lanes
                    s = jnp.where(other <= place, s, -1e30)
                pieces.append(s)
            most = functools.reduce(jnp.maximum, pieces)
            old = top[here, :]
            new = jnp.maximum(old, jnp.max(most, axis=1, keepdims=True))
            shrink = jnp.exp(old - new)
            raised = [jnp.exp(s - new) for s in pieces]
            total[here, :] = total[here, :] * shrink + functools.reduce(jnp.add, raised)
            weights = jnp.concatenate([r.astype(jnp.bfloat16) for r in raised], axis=1)
            summed[here, :] = summed[here, :] * shrink + jnp.dot(
                weights, keys, preferred_element_type=jnp.float32
            )
            top[here, :] = new

    attend(sp, True)

    def earlier(slot):
        @pl.when(slot < sp)
        def _():
            attend(slot, False)

    def slots(step):
        up_from = lax.rem(chip + chips - step, chips)
        down_from = lax.rem(chip + step, chips)
        return up_from, down_from

    def arrive(slot, step, way, part, target, send):
        hop(slot, step, way, part, target).wait_recv()
        if send is True:
            hop(slot, step, way, part, target).start()
        elif send is not False:

            @pl.when(send)
            def _():
                hop(slot, step, way, part, target).start()

    def partner(step, way, slot):
        share(slot, step, way).wait_recv()
        earlier(slot)

    def both(step):
        up_from, down_from = slots(step)
        before_up, before_down = slots(step - 1)
        up_slot, down_slot = up_from * 2 + core, down_from * 2 + core
        for part in range(2):
            arrive(up_slot, step, 0, part, up_sp, step < ups)
        share(up_slot, step, 0).start()
        earlier(up_slot)
        for part in range(2):
            arrive(down_slot, step, 1, part, down_sp, step < downs)
        share(down_slot, step, 1).start()
        earlier(down_slot)
        partner(step - 1, 0, before_up * 2 + 1 - core)

        @pl.when(step >= 2)
        def _():
            partner(step - 1, 1, before_down * 2 + 1 - core)

    if downs >= 1:
        lax.fori_loop(1, downs + 1, lambda i, c: (both(i), c)[1], 0)
    last_up, last_down = slots(downs)
    up_from, _ = slots(ups)
    up_slot = up_from * 2 + core
    for part in range(2):
        arrive(up_slot, ups, 0, part, up_sp, False)
    share(up_slot, ups, 0).start()
    earlier(up_slot)
    partner(downs, 0, last_up * 2 + 1 - core)
    if downs >= 1:
        partner(downs, 1, last_down * 2 + 1 - core)
    partner(ups, 0, up_from * 2 + 1 - core)

    def finished(lo):
        here = slice(lo, lo + half)
        whole = jnp.sum(total[here, :], axis=1, keepdims=True)
        return summed[here, :] / whole

    left = pltpu.roll(finished(0), size, 1)
    right = finished(half)
    lane = lax.broadcasted_iota(jnp.int32, left.shape, 1)
    att_all[tp] = jnp.where(lane < size, left, right).astype(jnp.bfloat16)

    def give(d):
        return remote(
            att_all.at[tp],
            att_all.at[tp],
            att_send.at[d],
            att_recv.at[tp],
            tp=lax.rem(tp + d, tp_size),
        )

    def take(d):
        owner = lax.rem(tp + tp_size - d, tp_size)
        return remote(
            att_all.at[owner],
            att_all.at[owner],
            att_send.at[d],
            att_recv.at[owner],
            tp=owner,
        )

    for d in range(1, tp_size):
        give(d).start()
    for d in range(1, tp_size):
        take(d).wait_recv()
    projected = jnp.zeros((half, wide.shape[1]), jnp.float32)
    for j in range(tp_size // 2):
        pair = jnp.concatenate([att_all[2 * j], att_all[2 * j + 1]], axis=1)
        projected += jnp.dot(
            pair, wide[j * 4 * size : (j + 1) * 4 * size, :], preferred_element_type=jnp.float32
        )
    columns = weight_ref.shape[1]
    for part in range(2):
        here = slice(part * half, (part + 1) * half)
        mixed_ref[here, :] = (
            residual_ref[here, :].astype(jnp.float32)
            + projected[:, part * columns : (part + 1) * columns]
        ).astype(jnp.bfloat16)

    if ups >= 1:
        for step in range(ups):
            for part in range(2):
                hop(sp, step, 0, part, up_sp).wait_send()
        for step in range(downs):
            for part in range(2):
                hop(sp, step, 1, part, down_sp).wait_send()
        for step in range(1, ups + 1):
            share(sp, step, 0).wait_send()
        for step in range(1, downs + 1):
            share(sp, step, 1).wait_send()
    share(sp, 0, 0).wait_send()
    for d in range(1, tp_size):
        give(d).wait_send()


def attention(mesh, query_rows, key_rows, value_rows, cum_gates, residual, output_weight):
    sp_size, tp_size = mesh.shape["sp"], mesh.shape["tp"]
    rows, size = query_rows.shape
    columns = output_weight.shape[1]
    vmem = pl.BlockSpec(memory_space=pltpu.VMEM)
    chips = sp_size // 2
    steps = chips // 2 + 1
    return pl.pallas_call(
        functools.partial(attention_kernel, sp_size, tp_size),
        out_shape=jax.ShapeDtypeStruct((rows, columns), jnp.bfloat16),
        in_specs=[vmem] * 6,
        out_specs=vmem,
        scratch_shapes=[
            pltpu.VMEM((sp_size, GATE_ROWS + rows, 2 * size), jnp.bfloat16),
            pltpu.VMEM((rows, 2 * size), jnp.bfloat16),
            pltpu.VMEM((tp_size * 2 * size, 2 * columns), jnp.bfloat16),
            pltpu.VMEM((rows, 2 * size), jnp.float32),
            pltpu.VMEM((rows, 2 * size), jnp.float32),
            pltpu.VMEM((rows, 2 * size), jnp.float32),
            pltpu.VMEM((tp_size, rows // 2, 2 * size), jnp.bfloat16),
            pltpu.SemaphoreType.DMA((sp_size, 2)),
            pltpu.SemaphoreType.DMA((sp_size,)),
            pltpu.SemaphoreType.DMA((steps, 2, 2)),
            pltpu.SemaphoreType.DMA((steps, 2)),
            pltpu.SemaphoreType.DMA((tp_size,)),
            pltpu.SemaphoreType.DMA((tp_size,)),
        ],
        compiler_params=pltpu.CompilerParams(
            collective_id=0, has_side_effects=True, vmem_limit_bytes=40 << 20
        ),
        cost_estimate=pl.CostEstimate(
            flops=4 * rows * rows * sp_size * 2 * size,
            bytes_accessed=1 << 22,
            transcendentals=rows * rows * sp_size,
        ),
    )(
        query_rows,
        key_rows,
        value_rows,
        cum_gates.reshape(4, rows // 4),
        residual,
        output_weight,
    )


def normalize(rows, norm_gain):
    wide = rows.astype(jnp.float32)
    factor = lax.rsqrt(jnp.mean(wide * wide, axis=-1, keepdims=True) + NORM_EPS)
    return (wide * factor * norm_gain.astype(jnp.float32)).astype(jnp.bfloat16)


def body(
    mesh,
    query_rows,
    key_rows,
    value_rows,
    cum_gates,
    residual,
    output_weight,
    norm_gain,
    expert_index,
    route_weights,
    gate_weight,
    up_weight,
    down_weight,
):
    mixed = attention(
        mesh, query_rows, key_rows, value_rows, cum_gates, residual, output_weight
    )
    rows = residual.shape[0]
    topk = expert_index.shape[1]
    local_experts = gate_weight.shape[0]
    groups = lax.axis_size("sp")
    experts = local_experts * groups
    capacity = 2 * rows * topk // experts
    chosen = expert_index.reshape(rows * topk)
    matches = (chosen[:, None] == jnp.arange(experts, dtype=jnp.int32)[None, :]).astype(jnp.int32)
    rank = jnp.sum((jnp.cumsum(matches, axis=0) - matches) * matches, axis=1)
    slot = chosen * capacity + rank
    owner = jnp.arange(rows * topk, dtype=jnp.int32) // topk
    slot_token = jnp.full((experts * capacity,), rows, jnp.int32).at[slot].set(owner)
    padded = jnp.concatenate([mixed, jnp.zeros((1, mixed.shape[1]), mixed.dtype)], axis=0)
    outgoing = padded[slot_token].reshape(experts, capacity, mixed.shape[1])
    arrived = lax.all_to_all(outgoing, "sp", split_axis=0, concat_axis=0, tiled=True)
    count = arrived.shape[1]
    grouped = arrived.reshape(groups, local_experts, count, arrived.shape[2])
    normed = normalize(lax.all_gather(grouped, "tp", axis=3, tiled=True), norm_gain)
    gate_input = jnp.einsum(
        "seid,edf->seif", normed, gate_weight, preferred_element_type=jnp.float32
    )
    linear_input = jnp.einsum(
        "seid,edf->seif", normed, up_weight, preferred_element_type=jnp.float32
    )
    gate_cut = jnp.minimum(gate_input, CLAMP_LIMIT)
    linear_cut = jnp.clip(linear_input, -CLAMP_LIMIT, CLAMP_LIMIT)
    activated = (gate_cut * jax.nn.sigmoid(SILU_ALPHA * gate_cut) * (linear_cut + 1.0)).astype(
        jnp.bfloat16
    )
    weight_rows = down_weight
    produced = jnp.einsum(
        "seif,efc->seic",
        lax.all_gather(activated, "tp", axis=3, tiled=True),
        weight_rows,
        preferred_element_type=jnp.float32,
    ).astype(jnp.bfloat16)
    returned = lax.all_to_all(
        produced.reshape(groups * local_experts, count, down_weight.shape[2]),
        "sp",
        split_axis=0,
        concat_axis=0,
        tiled=True,
    )
    flat = returned.reshape(experts * capacity, returned.shape[2])
    picked = flat[slot].reshape(rows, topk, flat.shape[1]).astype(jnp.float32)
    blended = jnp.sum(route_weights[:, :, None] * picked, axis=1)
    return (mixed.astype(jnp.float32) + blended).astype(jnp.bfloat16)


def solution(mesh):
    placed = (
        P("sp", "tp"),
        P("sp", "tp"),
        P("sp", "tp"),
        P("sp", "tp"),
        P("sp", "tp"),
        P(None, "tp"),
        P(),
        P("sp", None),
        P("sp", None),
        P("sp", None, "tp"),
        P("sp", None, "tp"),
        P("sp", None, "tp"),
    )
    return jax.shard_map(
        functools.partial(body, mesh), mesh=mesh, in_specs=placed, out_specs=P("sp", "tp"), check_vma=False)
```

time: 571 us -> 401 us (0.70)
  matrix products: 115 us -> 12.5 us
  Pallas kernels: 0 us -> 69.6 us
  waiting for transfers between devices: 267 us -> 207 us
  other arithmetic: 63 us -> 18.6 us
  starting transfers between devices: 37.2 us -> 14.6 us
  local copies, waits for them, and re-layouts: 28 us -> 21.7 us
    dot_general x65 -> x0, matrix products: 102 us -> none  [the longest x32 61.4 us: one_block(): jnp.einsum('qhk,khd->qhd', raised.astype(jnp.bfloat16), value_block, pref...]
    pallas_call x0 -> x1, Pallas kernels: none -> 69.6 us  [attention(): pl.pallas_call(functools.partial(attention_kernel, sp_size, tp_size), out...]
    all_gather x1 -> x0, waiting for transfers between devices: 48.4 us -> none  [side_by_side(): result = lax.all_gather(both, axis, axis=dim, tiled=True)]
    add x65 -> x0, other arithmetic: 36.8 us -> none  [the longest x32 36.7 us: one_block(): total = total * shrink + jnp.sum(raised, axis=-1)]
    all_to_all x2 -> x0, starting transfers between devices: 22.6 us -> none  [copy_for_each(): return lax.all_to_all(copies, axis, split_axis=0, concat_axis=0, tiled=True)]
    all_to_all x2 -> x0, waiting for transfers between devices: 12 us -> none  [copy_for_each(): return lax.all_to_all(copies, axis, split_axis=0, concat_axis=0, tiled=True)]
    split x1 -> x0, local copies, waits for them, and re-layouts: 7.28 us -> none  [side_by_side(): jnp.split(result, [sum(widths[:k]) for k in range(1, len(widths))], axis=...]
    reduce_sum x32 -> x0, other arithmetic: 6.28 us -> none  [one_block(): total = total * shrink + jnp.sum(raised, axis=-1)]
  transfers between devices with their start and end apart: 6 -> 3, of which waited for: 5 -> 3; matrix products, arithmetic and copies ran while one was open for 3% -> 0% of each run, Pallas kernels for 0% -> 0%
where the time goes in v1:
time: 401 us; the launch traced here: 399 us
  waiting for transfers between devices  207 us (52%)
  Pallas kernels  69.6 us (17%)
  blocking collectives  41.7 us (10%)
  local copies, waits for them, and re-layouts  21.7 us (5%)
  other arithmetic  18.6 us (5%)
  starting transfers between devices  14.6 us (4%)
  between operations  13.6 us (3%)
  matrix products  12.5 us (3%)
    all_gather x1, waiting for transfers between devices, body(): lax.all_gather(activated, 'tp', axis=3, tiled=True)  92.1 us
    all_gather x1, waiting for transfers between devices, body(): lax.all_gather(grouped, 'tp', axis=3, tiled=True)  81.2 us
    pallas_call x1, Pallas kernels, attention(): pl.pallas_call(functools.partial(attention_kernel, sp_size, tp_size), out...  69.6 us
    all_to_all x1, blocking collectives, body(): lax.all_to_all(outgoing, 'sp', split_axis=0, concat_axis=0, tiled=True)  41.7 us
    all_to_all x1, waiting for transfers between devices, body(): lax.all_to_all(produced.reshape(groups * local_experts, count, down_weigh...  33.3 us
    all_to_all x1, starting transfers between devices, body(): lax.all_to_all(produced.reshape(groups * local_experts, count, down_weigh...  14.4 us
    another operation x3, other arithmetic  9.15 us
  transfers between devices with their start and end apart: 3, of which 3 were waited for; matrix products, arithmetic and copies ran while one was open for 0% of the time, Pallas kernels for 0%

profile of v1, /device:TPU:25, one launch (start us, length us, event | category | flops | bytes accessed | tf_op | source)
XLA Modules:
  0.0 399.1 jit_solution(14431805353310632867)
XLA Ops:
  6.5 0.0 copy-start
  6.5 0.0 all-gather.6.cloned.1.call-start
  6.5 0.9 copy.22
  7.4 0.2 eq.29
  7.6 0.2 eq.25
  7.8 0.7 broadcast_multiply_fusion
  8.5 9.0 %reduce-window.6 = s32[32,8,128]{2,1,0:T(8,128)S(1)} reduce-window(s32[32,8,128]{2,1,0:T(8,128)S(1)} %fusion.41, s32[]{:T(128)} %constant.14.clone.1), window={size=1x1x128 pad=0_0x0_0x127_0}, to_apply=%region_0.0 | reduce-window | flops 4161536 | bytes 262148 | tf_op jit(solution)/shard_map/reduce-window
  17.5 0.1 slice.12
  17.6 0.1 copy.24
  17.8 0.1 copy.25
  17.8 0.1 broadcast_add_fusion
  17.9 0.1 copy.21
  18.1 0.2 mul.61
  18.4 4.3 %scatter_custom_fusion = s32[2048]{0:T(1024)S(1)} fusion(s32[1024]{0:T(1024)S(1)} %bitcast.103, s32[1024]{0:T(1024)S(1)} %add_select_fusion, s32[]{:T(128)} %constant.16.clone.1), kind=kCustom, calls=%fused_computation.45 | custom fusion | bytes 8196 | tf_op jit(solution)/shard_map/scatter | solution.py:368
  22.7 1.0 copy.17.q_ref
  23.7 1.0 copy.18.k_ref
  24.6 1.0 copy.19.v_ref
  25.6 0.0 copy-start.1
  25.6 0.9 copy-done.1
  26.5 0.0 copy-start.2
  26.5 0.9 copy-done.2
  27.5 0.7 copy-done.3
  28.1 69.6 %shard_map.118 = bf16[512,128]{1,0:T(8,128)(2,1)S(1)} custom-call(bf16[512,64]{1,0:T(8,128)(2,1)S(1)} %copy.17.q_ref, bf16[512,64]{1,0:T(8,128)(2,1)S(1)} %copy.18.k_ref, bf16[512,64]{1,0:T(8,128)(2,1)S(1)} %copy.19.v_ref, f32[4,128]{1,0:T(4,128)S(1)} %bitcast.96, bf16[512,128]{1,0:T(8,128)(2,1)S(1)} %copy-done.2, bf16[1024,128]{1,0:T(8,128)(2,1)S(1)} %copy-done.1), custom_call_target="tpu_custom_call" | custom-call | flops 4294967296 | bytes 4194304 | tf_op jit(solution)/shard_map/pallas_call | solution.py:295
  97.8 6.2 %gather_fusion = bf16[2048,128]{1,0:T(8,128)(2,1)S(1)} fusion(bf16[513,128]{1,0:T(8,128)(2,1)S(1)} %concatenate.3, s32[2048]{0:T(1024)S(1)} %fusion.42), kind=kCustom, calls=%fused_computation | custom fusion | bytes 1056768 | tf_op jit(solution)/shard_map/gather | solution.py:370
  104.0 41.7 %all_to_all.10 = bf16[32,64,128]{2,1,0:T(8,128)(2,1)} all-to-all(bf16[32,64,128]{2,1,0:T(8,128)(2,1)S(1)} %bitcast.98), channel_id=1, replica_groups=mesh['sp'=32,'tp'=16] {'sp'}, dimensions={0} | all-to-all | bytes 1048576 | tf_op jit(solution)/shard_map/all_to_all | solution.py:371
  145.7 0.0 all-gather.6.cloned.1.call-update
  145.7 0.2 all-gather.4.cloned.1.call-start
  145.9 0.0 copy-done.6
  146.0 81.2 %all-gather.6.cloned.1.call-done = bf16[32,64,2048]{2,1,0:T(8,128)(2,1)} async-done(((bf16[32,64,128]{2,1,0:T(8,128)(2,1)}), bf16[32,64,2048]{2,1,0:T(8,128)(2,1)}) %all-gather.6.cloned.1.call-update) | async-done | bytes 8388624 | tf_op jit(solution)/shard_map/all_gather | solution.py:374
  227.2 5.2 %fusion = f32[32,64]{1,0:T(8,128)S(1)} fusion(bf16[32,64,2048]{2,1,0:T(8,128)(2,1)} %all-gather.6.cloned.1.call-done), kind=kLoop, calls=%fused_computation.5 | loop fusion | flops 12580864 | bytes 8396800 | tf_op jit(solution)/shard_map/reduce_sum | solution.py:335
  232.4 0.0 copy-done
  232.4 0.5 copy-done.4
  232.9 2.5 fusion.13
  235.4 0.0 copy-done.7
  235.4 0.0 copy-start.8
  235.5 3.4 fusion.28
  238.9 0.0 all-gather.4.cloned.1.call-update
  238.9 0.0 copy-start.5
  238.9 92.1 %all-gather.4.cloned.1.call-done = bf16[32,1,64,2048]{3,2,0,1:T(8,128)(2,1)} async-done(((bf16[32,1,64,128]{3,2,0,1:T(8,128)(2,1)}), bf16[32,1,64,2048]{3,2,0,1:T(8,128)(2,1)}) %all-gather.4.cloned.1.call-update) | async-done | bytes 8388624 | tf_op jit(solution)/shard_map/all_gather | solution.py:389
  331.1 0.0 copy-done.8
  331.1 6.6 %fusion.31 = bf16[32,64,128]{2,1,0:T(8,128)(2,1)} fusion(bf16[32,1,64,2048]{3,2,0,1:T(8,128)(2,1)} %all-gather.4.cloned.1.call-done, bf16[1,2048,128]{2,1,0:T(8,128)(2,1)S(1)} %copy-done.8), kind=kOutput, calls=%fused_computation.20 | convolution fusion | flops 1074003968 | bytes 9437184 | tf_op jit(solution)/shard_map/seif,efc->seic/dot_general | solution.py:387
  337.6 14.4 %all-to-all-start.1 = ((bf16[32,64,128]{2,1,0:T(8,128)(2,1)}), bf16[32,64,128]{2,1,0:T(8,128)(2,1)S(1)}, u32[]{:S(2)}, u32[]{:S(2)}) async-start(bf16[32,64,128]{2,1,0:T(8,128)(2,1)} %fusion.31), calls=%async_computation.1 | async-start | bytes 1048576 | tf_op jit(solution)/shard_map/all_to_all | solution.py:393
  352.0 0.0 copy-done.5
  352.0 0.1 copy.20
  352.2 33.3 %all-to-all-done.1 = bf16[32,64,128]{2,1,0:T(8,128)(2,1)S(1)} async-done(((bf16[32,64,128]{2,1,0:T(8,128)(2,1)}), bf16[32,64,128]{2,1,0:T(8,128)(2,1)S(1)}, u32[]{:S(2)}, u32[]{:S(2)}) %all-to-all-start.1) | async-done | bytes 524320 | tf_op jit(solution)/shard_map/all_to_all | solution.py:393
  385.6 3.2 gather_fusion.1
  388.8 2.8 fusion.34
  391.6 0.7 add_convert_fusion
  (15 shorter events, 0.1 us)
Async XLA Ops:
  6.5 225.9 %copy-start = (bf16[1,2048,128]{2,1,0:T(8,128)(2,1)S(1)}, bf16[1,2048,128]{2,1,0:T(8,128)(2,1)}, u32[]{:S(2)}) copy-start(bf16[1,2048,128]{2,1,0:T(8,128)(2,1)} %param.21) | copy-start | bytes 1572868
  6.5 220.6 %all-gather.6.cloned.1.call-start = ((), (), s32[]{:S(2)}) async-start(), calls=%async_computation.3 | async-start | bytes 8912896 | tf_op jit(solution)/shard_map/all_gather | solution.py:374
  25.6 1.0 copy-start.1
  26.5 0.9 copy-start.2
  27.4 0.7 copy-start.3
  28.1 117.8 %copy-start.6 = (bf16[2048]{0:T(1024)(128)(2,1)S(1)}, bf16[2048]{0:T(1024)(128)(2,1)}, u32[]{:S(2)}) copy-start(bf16[2048]{0:T(1024)(128)(2,1)} %param.18) | copy-start | bytes 12292
  145.7 185.4 %all-gather.4.cloned.1.call-start = ((), (), s32[]{:S(2)}) async-start(), calls=%async_computation.2 | async-start | bytes 8912896 | tf_op jit(solution)/shard_map/all_gather | solution.py:389
  227.2 5.8 %copy-start.4 = (bf16[32,64,2048]{2,1,0:T(8,128)(2,1)S(1)}, bf16[32,64,2048]{2,1,0:T(8,128)(2,1)}, u32[]{:S(2)}) copy-start(bf16[32,64,2048]{2,1,0:T(8,128)(2,1)} %all-gather.6.cloned.1.call-done) | copy-start | bytes 25165828
  232.9 2.5 copy-start.7
  235.4 95.6 %copy-start.8 = (bf16[1,2048,128]{2,1,0:T(8,128)(2,1)S(1)}, bf16[1,2048,128]{2,1,0:T(8,128)(2,1)}, u32[]{:S(2)}) copy-start(bf16[1,2048,128]{2,1,0:T(8,128)(2,1)} %param.23) | copy-start | bytes 1572868
  238.9 113.1 %copy-start.5 = (f32[512,2]{0,1:T(2,128)S(1)}, f32[512,2]{0,1:T(2,128)}, u32[]{:S(2)}) copy-start(f32[512,2]{0,1:T(2,128)} %param.20) | copy-start | bytes 12292
  337.6 47.9 %all-to-all-start.1 = ((bf16[32,64,128]{2,1,0:T(8,128)(2,1)}), bf16[32,64,128]{2,1,0:T(8,128)(2,1)S(1)}, u32[]{:S(2)}, u32[]{:S(2)}) async-start(bf16[32,64,128]{2,1,0:T(8,128)(2,1)} %fusion.31), calls=%async_computation.1 | async-start | bytes 1048576 | tf_op jit(solution)/shard_map/all_to_all | solution.py:393
Sparse Core Ops, SparseCore 0:
  145.8 81.3 all-gather.5
  239.0 91.9 all-gather.3

commit v2 on v1

--- a/solution.py
+++ b/solution.py
@@ -26,16 +26,64 @@
     )
 
 
+def ring_start(n, place, make):
+    if n == 4:
+        for k in range(2):
+            make(place, k, 1, 0, k).start()
+            make(place, 1 - k, 3, 1, k).start()
+    elif n == 2:
+        for k in range(2):
+            make(place, k, 1, 0, k).start()
+
+
+def ring_forward(n, place, make):
+    if n == 4:
+        before, after = lax.rem(place + 3, 4), lax.rem(place + 1, 4)
+        make(before, 0, 1, 0, 2).wait_recv()
+        make(before, 0, 1, 0, 2).start()
+        make(after, 1, 3, 1, 2).wait_recv()
+        make(after, 1, 3, 1, 2).start()
+
+
+def ring_finish(n, place, make):
+    if n == 4:
+        make(lax.rem(place + 3, 4), 1, 1, 0, 0).wait_recv()
+        make(lax.rem(place + 1, 4), 0, 1, 0, 0).wait_recv()
+        for k in range(2):
+            make(lax.rem(place + 2, 4), k, 1, 0, 0).wait_recv()
+    elif n == 2:
+        for k in range(2):
+            make(1 - place, k, 1, 0, 0).wait_recv()
+
+
+def ring_sent(n, place, make):
+    if n == 4:
+        for k in range(3):
+            half = k if k < 2 else 0
+            make(place, half, 1, 0, k).wait_send()
+            make(place, 1 - half, 3, 1, k).wait_send()
+    elif n == 2:
+        for k in range(2):
+            make(place, k, 1, 0, k).wait_send()
+
+
 def attention_kernel(
     sp_size,
     tp_size,
+    y_size,
     q_ref,
     k_ref,
     v_ref,
     gate_ref,
     residual_ref,
     weight_ref,
+    gate_w,
+    up_w,
+    down_w,
     mixed_ref,
+    gate_all,
+    up_all,
+    down_all,
     kv_all,
     qpad,
     wide,
@@ -49,6 +97,9 @@
     pair_send,
     att_recv,
     att_send,
+    own_w,
+    w_recv,
+    w_send,
 ):
     chips = sp_size // 2
     ups = chips // 2
@@ -114,12 +165,42 @@
             sp=pair_sp,
         )
 
+    x_size = tp_size // y_size
+    y = tp // x_size
+    x = tp - y * x_size
+    matrices = ((gate_w, gate_all), (up_w, up_all), (down_w, down_all))
+    depth = gate_w.shape[1]
+
+    def weight_copy(m):
+        own, every = matrices[m]
+
+        def make(owner, k, step, way, index):
+            here = every.at[owner, pl.ds(k * (depth // 2), depth // 2), :]
+            mine = own.at[0, pl.ds(k * (depth // 2), depth // 2), :]
+            return remote(
+                mine if index < 2 else here,
+                here,
+                w_send.at[m, way, index],
+                w_recv.at[m, owner, k],
+                tp=lax.rem(y + step, y_size) * x_size + x,
+            )
+
+        return make
+
+    locals_w = [
+        pltpu.make_async_copy(own.at[0], every.at[y], own_w.at[m])
+        for m, (own, every) in enumerate(matrices)
+    ]
+
     if ups >= 1:
         for part in range(2):
             hop(sp, 0, 0, part, up_sp).start()
             if downs >= 1:
                 hop(sp, 0, 1, part, down_sp).start()
     share(sp, 0, 0).start()
+    for m in range(3):
+        ring_start(y_size, y, weight_copy(m))
+        locals_w[m].start()
 
     wide[...] = jnp.zeros_like(wide)
     for h in range(tp_size):
@@ -204,6 +285,11 @@
         earlier(down_slot)
         partner(step - 1, 0, before_up * 2 + 1 - core)
 
+        @pl.when(step == max(1, downs - 2))
+        def _():
+            for m in range(3):
+                ring_forward(y_size, y, weight_copy(m))
+
         @pl.when(step >= 2)
         def _():
             partner(step - 1, 1, before_down * 2 + 1 - core)
@@ -268,6 +354,13 @@
             residual_ref[here, :].astype(jnp.float32)
             + projected[:, part * columns : (part + 1) * columns]
         ).astype(jnp.bfloat16)
+
+    for m in range(3):
+        if downs < 1:
+            ring_forward(y_size, y, weight_copy(m))
+        ring_finish(y_size, y, weight_copy(m))
+        ring_sent(y_size, y, weight_copy(m))
+        locals_w[m].wait()
 
     if ups >= 1:
         for step in range(ups):
@@ -285,18 +378,39 @@
         give(d).wait_send()
 
 
-def attention(mesh, query_rows, key_rows, value_rows, cum_gates, residual, output_weight):
+def y_of(tp_size):
+    return math.isqrt(tp_size)
+
+
+def attention(
+    mesh,
+    query_rows,
+    key_rows,
+    value_rows,
+    cum_gates,
+    residual,
+    output_weight,
+    gate_weight,
+    up_weight,
+    down_weight,
+):
     sp_size, tp_size = mesh.shape["sp"], mesh.shape["tp"]
     rows, size = query_rows.shape
     columns = output_weight.shape[1]
     vmem = pl.BlockSpec(memory_space=pltpu.VMEM)
+    anywhere = pl.BlockSpec(memory_space=pl.ANY)
+    y_size = y_of(tp_size)
     chips = sp_size // 2
     steps = chips // 2 + 1
     return pl.pallas_call(
-        functools.partial(attention_kernel, sp_size, tp_size),
-        out_shape=jax.ShapeDtypeStruct((rows, columns), jnp.bfloat16),
-        in_specs=[vmem] * 6,
-        out_specs=vmem,
+        functools.partial(attention_kernel, sp_size, tp_size, y_size),
+        out_shape=[jax.ShapeDtypeStruct((rows, columns), jnp.bfloat16)]
+        + [
+            jax.ShapeDtypeStruct((y_size, *w.shape[1:]), jnp.bfloat16)
+            for w in (gate_weight, up_weight, down_weight)
+        ],
+        in_specs=[vmem] * 6 + [anywhere] * 3,
+        out_specs=[vmem] + [anywhere] * 3,
         scratch_shapes=[
             pltpu.VMEM((sp_size, GATE_ROWS + rows, 2 * size), jnp.bfloat16),
             pltpu.VMEM((rows, 2 * size), jnp.bfloat16),
@@ -311,6 +425,9 @@
             pltpu.SemaphoreType.DMA((steps, 2)),
             pltpu.SemaphoreType.DMA((tp_size,)),
             pltpu.SemaphoreType.DMA((tp_size,)),
+            pltpu.SemaphoreType.DMA((3,)),
+            pltpu.SemaphoreType.DMA((3, y_size, 2)),
+            pltpu.SemaphoreType.DMA((3, 2, 3)),
         ],
         compiler_params=pltpu.CompilerParams(
             collective_id=0, has_side_effects=True, vmem_limit_bytes=40 << 20
@@ -327,13 +444,391 @@
         cum_gates.reshape(4, rows // 4),
         residual,
         output_weight,
+        gate_weight,
+        up_weight,
+        down_weight,
     )
 
 
-def normalize(rows, norm_gain):
-    wide = rows.astype(jnp.float32)
-    factor = lax.rsqrt(jnp.mean(wide * wide, axis=-1, keepdims=True) + NORM_EPS)
-    return (wide * factor * norm_gain.astype(jnp.float32)).astype(jnp.bfloat16)
+CAP = 64
+
+
+def expert_kernel(
+    sp_size,
+    tp_size,
+    y_size,
+    mixed_ref,
+    slot_row,
+    slot_col,
+    route_ref,
+    gain_ref,
+    gate_all,
+    up_all,
+    down_all,
+    out_ref,
+    outgoing,
+    landed,
+    tokens,
+    normed,
+    gate_v,
+    up_v,
+    down_v,
+    hidden,
+    produced,
+    turned,
+    returned,
+    load_sem,
+    z_send,
+    z_recv,
+    t_send,
+    t_recv,
+    h_send,
+    h_recv,
+    y_send,
+    y_recv,
+    r_send,
+    r_recv,
+):
+    x_size = tp_size // y_size
+    chips = sp_size // 2
+    sp = lax.axis_index("sp")
+    tp = lax.axis_index("tp")
+    y = tp // x_size
+    x = tp - y * x_size
+    chip = sp // 2
+    core = sp - 2 * chip
+    rows, columns = mixed_ref.shape
+    group = sp_size // y_size
+    chunks = 2
+    blocks = group // chunks
+    height = blocks * CAP
+    width = tp_size * columns
+    hid = y_size * columns
+
+    barrier = pltpu.get_barrier_semaphore()
+    for d in range(1, sp_size):
+        pl.semaphore_signal(
+            barrier, inc=1, device_id={"sp": lax.rem(sp + d, sp_size)}, device_id_type=MESH
+        )
+    for d in range(1, tp_size):
+        pl.semaphore_signal(
+            barrier, inc=1, device_id={"tp": lax.rem(tp + d, tp_size)}, device_id_type=MESH
+        )
+    loads = []
+    for m, (source, target) in enumerate(((gate_all, gate_v), (up_all, up_v), (down_all, down_v))):
+        for k in range(y_size):
+            loads.append(
+                pltpu.make_async_copy(
+                    source.at[k],
+                    target.at[:, pl.ds(k * columns, columns)],
+                    load_sem.at[m, k],
+                )
+            )
+    for load in loads:
+        load.start()
+
+    mixed = mixed_ref[...]
+    batch = min(4, sp_size)
+    first, second = slot_row[0:1, :], slot_row[1:2, :]
+    for c in range(sp_size // batch):
+        number = lax.broadcasted_iota(jnp.int32, (batch * CAP, rows), 0) + c * batch * CAP
+        chosen = jnp.logical_or(number == first, number == second)
+        picked = jnp.dot(
+            chosen.astype(jnp.float32).astype(jnp.bfloat16),
+            mixed,
+            preferred_element_type=jnp.float32,
+        ).astype(jnp.bfloat16)
+        for b in range(batch):
+            outgoing[c * batch + b] = picked[b * CAP : (b + 1) * CAP]
+    landed[sp] = outgoing[sp]
+    pl.semaphore_wait(barrier, sp_size - 1 + tp_size - 1)
+
+    def near(i):
+        j = i // 2
+        far = (j + 1) // 2
+        odd = j - 2 * (j // 2)
+        chip_there = lax.rem(chip + chips + (2 * odd - 1) * far, chips)
+        other = i - 2 * j
+        return chip_there * 2 + core + other * (1 - 2 * core)
+
+    def send_z(i):
+        there = near(i)
+        return remote(
+            outgoing.at[there], landed.at[sp], z_send.at[i], z_recv.at[sp], sp=there
+        )
+
+    def take_z(source):
+        return remote(outgoing.at[sp], landed.at[source], z_send.at[0], z_recv.at[source], sp=source)
+
+    lax.fori_loop(1, sp_size, lambda i, c: (send_z(i).start(), c)[1], 0)
+
+    def give_t(i, d, source):
+        y_there = source // group
+        slot = source - y_there * group
+        return remote(
+            landed.at[source],
+            tokens.at[slot, tp],
+            t_send.at[i, d],
+            t_recv.at[slot],
+            tp=y_there * x_size + lax.rem(x + d, x_size),
+        )
+
+    def own_t(source):
+        slot = source - (source // group) * group
+        return pltpu.make_async_copy(landed.at[source], tokens.at[slot, tp], t_recv.at[slot])
+
+    def pass_on(i, source):
+        for d in range(1, x_size):
+            give_t(i, d, source).start()
+
+        @pl.when(source // group == y)
+        def _():
+            own_t(source).start()
+
+        @pl.when(source // group != y)
+        def _():
+            give_t(i, 0, source).start()
+
+    pass_on(0, sp)
+
+    def arrived(i):
+        source = near(i)
+        take_z(source).wait_recv()
+        pass_on(i, source)
+
+    lax.fori_loop(1, sp_size, lambda i, c: (arrived(i), c)[1], 0)
+
+    def h_copy(c):
+        def make(owner, k, step, way, index):
+            here = hidden.at[
+                pl.ds(k * (y_size // 2), y_size // 2), owner, pl.ds(c * height, height), :
+            ]
+            return remote(
+                here,
+                here,
+                h_send.at[c, way, index],
+                h_recv.at[c, owner, k],
+                tp=y * x_size + lax.rem(x + step, x_size),
+            )
+
+        return make
+
+    for load in loads[: 2 * y_size]:
+        load.wait()
+    for c in range(chunks):
+        for b in range(blocks):
+            slot = c * blocks + b
+            pltpu.make_async_copy(tokens.at[slot], tokens.at[slot], t_recv.at[slot]).wait()
+            squares = jnp.zeros((CAP, columns), jnp.float32)
+            for t in range(tp_size):
+                wide = tokens[slot, t].astype(jnp.float32)
+                squares += wide * wide
+            scale = lax.rsqrt(jnp.sum(squares, axis=1, keepdims=True) / width + NORM_EPS)
+            for t in range(tp_size):
+                wide = tokens[slot, t].astype(jnp.float32)
+                normed[slot * CAP : (slot + 1) * CAP, t * columns : (t + 1) * columns] = (
+                    wide * scale * gain_ref[t : t + 1, :]
+                ).astype(jnp.bfloat16)
+        here = slice(c * height, (c + 1) * height)
+        tile = min(256, hid)
+        for n in range(hid // tile):
+            cols = slice(n * tile, (n + 1) * tile)
+            gate_input = jnp.dot(normed[here, :], gate_v[:, cols], preferred_element_type=jnp.float32)
+            linear_input = jnp.dot(normed[here, :], up_v[:, cols], preferred_element_type=jnp.float32)
+            cut = jnp.minimum(gate_input, CLAMP_LIMIT)
+            linear = jnp.clip(linear_input, -CLAMP_LIMIT, CLAMP_LIMIT)
+            active = (cut / (1.0 + jnp.exp(-SILU_ALPHA * cut)) * (linear + 1.0)).astype(jnp.bfloat16)
+            for k in range(tile // columns):
+                hidden[n * (tile // columns) + k, x, here, :] = active[
+                    :, k * columns : (k + 1) * columns
+                ]
+        ring_start(x_size, x, h_copy(c))
+
+    def give_y(c, d):
+        y_there = lax.rem(y + d, y_size)
+        here = pl.ds(c * height, height)
+        return remote(
+            produced.at[y_there, here, :],
+            turned.at[y, here, :],
+            y_send.at[c, d],
+            y_recv.at[c, y],
+            tp=y_there * x_size + x,
+        )
+
+    def take_y(c, d):
+        source = lax.rem(y + y_size - d, y_size)
+        here = pl.ds(c * height, height)
+        return source, remote(
+            produced.at[source, here, :],
+            turned.at[source, here, :],
+            y_send.at[c, d],
+            y_recv.at[c, source],
+            tp=source * x_size + x,
+        )
+
+    def send_r(source, slot):
+        there = source * group + slot
+        return remote(
+            turned.at[source, pl.ds(slot * CAP, CAP), :],
+            returned.at[sp],
+            r_send.at[there],
+            r_recv.at[sp],
+            sp=there,
+        )
+
+    def give_back(source, c):
+        for b in range(blocks):
+            slot = c * blocks + b
+            there = source * group + slot
+
+            @pl.when(there == sp)
+            def _():
+                returned[sp] = turned[source, slot * CAP : (slot + 1) * CAP, :]
+
+            @pl.when(there != sp)
+            def _():
+                send_r(source, slot).start()
+
+    for load in loads[2 * y_size :]:
+        load.wait()
+    for c in range(chunks):
+        ring_forward(x_size, x, h_copy(c))
+    for c in range(chunks):
+        here = slice(c * height, (c + 1) * height)
+        ring_finish(x_size, x, h_copy(c))
+        made = jnp.zeros((height, hid), jnp.float32)
+        for t in range(0, tp_size, 2):
+            k, j = t // x_size, t % x_size
+            pair = jnp.concatenate([hidden[k, j, here, :], hidden[k, j + 1, here, :]], axis=1)
+            made += jnp.dot(
+                pair,
+                down_v[t * columns : (t + 2) * columns, :],
+                preferred_element_type=jnp.float32,
+            )
+        for k in range(y_size):
+            produced[k, here, :] = made[:, k * columns : (k + 1) * columns].astype(jnp.bfloat16)
+        for d in range(1, y_size):
+            give_y(c, d).start()
+        turned[y, here, :] = produced[y, here, :]
+        give_back(y, c)
+    for c in range(chunks):
+        for d in range(1, y_size):
+            source, copy = take_y(c, d)
+            copy.wait_recv()
+            give_back(source, c)
+
+    sums = [jnp.zeros((rows, columns), jnp.float32) for _ in range(2)]
+    for c in range(sp_size // batch):
+        for b in range(batch):
+            e = c * batch + b
+
+            @pl.when(sp != e)
+            def _():
+                remote(
+                    turned.at[0, pl.ds(0, CAP), :],
+                    returned.at[e],
+                    r_send.at[e],
+                    r_recv.at[e],
+                    sp=sp,
+                ).wait_recv()
+
+        block = jnp.concatenate([returned[c * batch + b] for b in range(batch)], axis=0)
+        number = lax.broadcasted_iota(jnp.int32, (rows, batch * CAP), 1) + c * batch * CAP
+        for k in range(2):
+            chosen = (number == slot_col[:, k : k + 1]).astype(jnp.float32).astype(jnp.bfloat16)
+            sums[k] += jnp.dot(chosen, block, preferred_element_type=jnp.float32)
+    blended = route_ref[:, 0:1] * sums[0] + route_ref[:, 1:2] * sums[1]
+    out_ref[...] = (mixed.astype(jnp.float32) + blended).astype(jnp.bfloat16)
+
+    for i in range(1, sp_size):
+        send_z(i).wait_send()
+    for i in range(sp_size):
+        for d in range(1, x_size):
+            give_t(i, d, sp).wait_send()
+
+        @pl.when(near(i) // group != y)
+        def _():
+            give_t(i, 0, sp).wait_send()
+
+    for c in range(chunks):
+        ring_sent(x_size, x, h_copy(c))
+        for d in range(1, y_size):
+            give_y(c, d).wait_send()
+    for e in range(sp_size):
+
+        @pl.when(sp != e)
+        def _():
+            send_r(e // group, e % group).wait_send()
+
+
+def experts(mesh, mixed, slot, route_weights, norm_gain, gate_all, up_all, down_all):
+    sp_size, tp_size = mesh.shape["sp"], mesh.shape["tp"]
+    y_size = y_of(tp_size)
+    x_size = tp_size // y_size
+    rows, columns = mixed.shape
+    group = sp_size // y_size
+    depth = gate_all.shape[1]
+    hid = y_size * columns
+    vmem = pl.BlockSpec(memory_space=pltpu.VMEM)
+    anywhere = pl.BlockSpec(memory_space=pl.ANY)
+    bf16 = jnp.bfloat16
+    dma = pltpu.SemaphoreType.DMA
+    return pl.pallas_call(
+        functools.partial(expert_kernel, sp_size, tp_size, y_size),
+        out_shape=jax.ShapeDtypeStruct((rows, columns), bf16),
+        in_specs=[vmem] * 5 + [anywhere] * 3,
+        out_specs=vmem,
+        scratch_shapes=[
+            pltpu.VMEM((sp_size, CAP, columns), bf16),
+            pltpu.VMEM((sp_size, CAP, columns), bf16),
+            pltpu.VMEM((group, tp_size, CAP, columns), bf16),
+            pltpu.VMEM((group * CAP, tp_size * columns), bf16),
+            pltpu.VMEM((depth, hid), bf16),
+            pltpu.VMEM((depth, hid), bf16),
+            pltpu.VMEM((depth, hid), bf16),
+            pltpu.VMEM((y_size, x_size, group * CAP, columns), bf16),
+            pltpu.VMEM((y_size, group * CAP, columns), bf16),
+            pltpu.VMEM((y_size, group * CAP, columns), bf16),
+            pltpu.VMEM((sp_size, CAP, columns), bf16),
+            dma((3, y_size)),
+            dma((sp_size,)),
+            dma((sp_size,)),
+            dma((sp_size, x_size)),
+            dma((group,)),
+            dma((2, 2, 3)),
+            dma((2, x_size, 2)),
+            dma((2, y_size)),
+            dma((2, y_size)),
+            dma((sp_size,)),
+            dma((sp_size,)),
+        ],
+        compiler_params=pltpu.CompilerParams(
+            collective_id=1, has_side_effects=True, vmem_limit_bytes=48 << 20
+        ),
+        cost_estimate=pl.CostEstimate(
+            flops=6 * group * CAP * depth * hid, bytes_accessed=1 << 23, transcendentals=1 << 18
+        ),
+    )(
+        mixed,
+        slot.T,
+        slot,
+        route_weights,
+        norm_gain.astype(jnp.float32).reshape(tp_size, columns),
+        gate_all,
+        up_all,
+        down_all,
+    )
+
+
+def slots_of(expert_index, count):
+    rows, topk = expert_index.shape
+    chosen = expert_index.reshape(rows * topk)
+    matches = chosen[:, None] == jnp.arange(count, dtype=jnp.int32)[None, :]
+    order = jnp.arange(rows * topk, dtype=jnp.int32)
+    before = (order[None, :] < order[:, None]).astype(jnp.bfloat16)
+    ahead = jnp.dot(before, matches.astype(jnp.bfloat16), preferred_element_type=jnp.float32)
+    rank = jnp.sum(jnp.where(matches, ahead, 0.0), axis=1).astype(jnp.int32)
+    return (chosen * CAP + rank).reshape(rows, topk)
 
 
 def body(
@@ -351,56 +846,20 @@
     up_weight,
     down_weight,
 ):
-    mixed = attention(
-        mesh, query_rows, key_rows, value_rows, cum_gates, residual, output_weight
+    slot = slots_of(expert_index, mesh.shape["sp"])
+    mixed, gate_all, up_all, down_all = attention(
+        mesh,
+        query_rows,
+        key_rows,
+        value_rows,
+        cum_gates,
+        residual,
+        output_weight,
+        gate_weight,
+        up_weight,
+        down_weight,
     )
-    rows = residual.shape[0]
-    topk = expert_index.shape[1]
-    local_experts = gate_weight.shape[0]
-    groups = lax.axis_size("sp")
-    experts = local_experts * groups
-    capacity = 2 * rows * topk // experts
-    chosen = expert_index.reshape(rows * topk)
-    matches = (chosen[:, None] == jnp.arange(experts, dtype=jnp.int32)[None, :]).astype(jnp.int32)
-    rank = jnp.sum((jnp.cumsum(matches, axis=0) - matches) * matches, axis=1)
-    slot = chosen * capacity + rank
-    owner = jnp.arange(rows * topk, dtype=jnp.int32) // topk
-    slot_token = jnp.full((experts * capacity,), rows, jnp.int32).at[slot].set(owner)
-    padded = jnp.concatenate([mixed, jnp.zeros((1, mixed.shape[1]), mixed.dtype)], axis=0)
-    outgoing = padded[slot_token].reshape(experts, capacity, mixed.shape[1])
-    arrived = lax.all_to_all(outgoing, "sp", split_axis=0, concat_axis=0, tiled=True)
-    count = arrived.shape[1]
-    grouped = arrived.reshape(groups, local_experts, count, arrived.shape[2])
-    normed = normalize(lax.all_gather(grouped, "tp", axis=3, tiled=True), norm_gain)
-    gate_input = jnp.einsum(
-        "seid,edf->seif", normed, gate_weight, preferred_element_type=jnp.float32
-    )
-    linear_input = jnp.einsum(
-        "seid,edf->seif", normed, up_weight, preferred_element_type=jnp.float32
-    )
-    gate_cut = jnp.minimum(gate_input, CLAMP_LIMIT)
-    linear_cut = jnp.clip(linear_input, -CLAMP_LIMIT, CLAMP_LIMIT)
-    activated = (gate_cut * jax.nn.sigmoid(SILU_ALPHA * gate_cut) * (linear_cut + 1.0)).astype(
-        jnp.bfloat16
-    )
-    weight_rows = down_weight
-    produced = jnp.einsum(
-        "seif,efc->seic",
-        lax.all_gather(activated, "tp", axis=3, tiled=True),
-        weight_rows,
-        preferred_element_type=jnp.float32,
-    ).astype(jnp.bfloat16)
-    returned = lax.all_to_all(
-        produced.reshape(groups * local_experts, count, down_weight.shape[2]),
-        "sp",
-        split_axis=0,
-        concat_axis=0,
-        tiled=True,
-    )
-    flat = returned.reshape(experts * capacity, returned.shape[2])
-    picked = flat[slot].reshape(rows, topk, flat.shape[1]).astype(jnp.float32)
-    blended = jnp.sum(route_weights[:, :, None] * picked, axis=1)
-    return (mixed.astype(jnp.float32) + blended).astype(jnp.bfloat16)
+    return experts(mesh, mixed, slot, route_weights, norm_gain, gate_all, up_all, down_all)
 
 
 def solution(mesh):
@@ -419,4 +878,9 @@
         P("sp", None, "tp"),
     )
     return jax.shard_map(
-        functools.partial(body, mesh), mesh=mesh, in_specs=placed, out_specs=P("sp", "tp"), check_vma=False)
+        functools.partial(body, mesh),
+        mesh=mesh,
+        in_specs=placed,
+        out_specs=P("sp", "tp"),
+        check_vma=False,
+    )

time: 401 us -> 193 us (0.48)
  waiting for transfers between devices: 207 us -> 0 us
  Pallas kernels: 69.6 us -> 178 us
  blocking collectives: 41.7 us -> 0 us
  other arithmetic: 18.6 us -> 0.04 us
  starting transfers between devices: 14.6 us -> 0 us
  between operations: 13.6 us -> 0.15 us
  matrix products: 12.5 us -> 0.54 us
  local copies, waits for them, and re-layouts: 21.7 us -> 14.4 us
    all_gather x2 -> x0, waiting for transfers between devices: 173 us -> none  [the longest x1 92.1 us: body(): lax.all_gather(activated, 'tp', axis=3, tiled=True)]
    pallas_call x1 -> x2, Pallas kernels: 69.6 us -> 178 us  [the longest x1 104 us: experts(): pl.pallas_call(functools.partial(expert_kernel, sp_size, tp_size, y_size)...]
    all_to_all x1 -> x0, blocking collectives: 41.7 us -> none  [body(): lax.all_to_all(outgoing, 'sp', split_axis=0, concat_axis=0, tiled=True)]
    all_to_all x1 -> x0, waiting for transfers between devices: 33.3 us -> none  [body(): lax.all_to_all(produced.reshape(groups * local_experts, count, down_weigh...]
    all_to_all x1 -> x0, starting transfers between devices: 14.4 us -> none  [body(): lax.all_to_all(produced.reshape(groups * local_experts, count, down_weigh...]
    dot_general x3 -> x1, matrix products: 12.5 us -> 0.54 us  [slots_of(): jnp.dot(before, matches.astype(jnp.bfloat16), preferred_element_type=jnp....]
    gather x2 -> x0, local copies, waits for them, and re-layouts: 9.38 us -> none  [the longest x1 6.18 us: body(): outgoing = padded[slot_token].reshape(experts, capacity, mixed.shape[1])]
    another operation x3 -> x0, other arithmetic: 9.15 us -> none
  transfers between devices with their start and end apart: 3 -> 0, of which waited for: 3 -> 0; matrix products, arithmetic and copies ran while one was open for 0% -> 0% of each run, Pallas kernels for 0% -> 0%
where the time goes in v2:
time: 193 us
  Pallas kernels  178 us (92%)
  local copies, waits for them, and re-layouts  14.4 us (7%)
    pallas_call x1, Pallas kernels, experts(): pl.pallas_call(functools.partial(expert_kernel, sp_size, tp_size, y_size)...  104 us
    pallas_call x1, Pallas kernels, attention(): pl.pallas_call(functools.partial(attention_kernel, sp_size, tp_size, y_si...  73.9 us
    unnamed x30, local copies, waits for them, and re-layouts  13.7 us

profile of v2, /device:TPU:25, one launch (start us, length us, event | category | flops | bytes accessed | tf_op | source)
XLA Modules:
  0.0 192.8 jit_solution(1895674936073847070)
XLA Ops:
  0.0 1.0 copy.28.q_ref
  1.0 1.0 copy.29.k_ref
  1.9 1.0 copy.30.v_ref
  2.9 0.0 copy-start
  2.9 1.0 copy-done
  3.9 0.0 copy-start.1
  3.9 1.0 copy-done.1
  5.0 0.0 copy-start.2
  5.0 1.0 copy-done.2
  6.0 0.0 copy-start.3
  6.0 0.9 copy-done.3
  7.0 0.0 copy-start.4
  7.0 0.9 copy-done.4
  7.9 0.0 copy-start.5
  7.9 0.7 copy-done.5
  8.6 0.0 copy-start.9
  8.6 73.9 %shard_map.118 = (bf16[512,128]{1,0:T(8,128)(2,1)S(1)}, bf16[4,2048,128]{2,1,0:T(8,128)(2,1)S(1)}, bf16[4,2048,128]{2,1,0:T(8,128)(2,1)S(1)}, bf16[4,2048,128]{2,1,0:T(8,128)(2,1)S(1)}) custom-call(bf16[512,64]{1,0:T(8,128)(2,1)S(1)} %copy.28.q_ref, bf16[512,64]{1,0:T(8,128)(2,1)S(1)} %copy.29.k_ref, bf16[512,64]{1,0:T(8,128)(2,1)S(1)} %copy.30.v_ref, ...), custom_call_target="tpu_custom_call" | custom-call | flops 4294967296 | bytes 4194304 | tf_op jit(solution)/shard_map/pallas_call | solution.py:405
  82.4 0.0 copy-start.6
  82.4 1.3 copy-done.6
  83.8 0.0 copy-start.8
  83.8 1.3 copy-done.8
  85.1 0.0 copy-start.10
  85.1 0.0 copy-start.11
  85.1 0.0 copy-done.9
  85.1 0.1 copy.31
  85.2 0.2 eq.15
  85.4 0.5 fusion.2
  86.0 0.2 convert_element_type.11
  86.2 0.1 copy.32
  86.4 0.1 copy.33.slot_row
  86.5 0.0 copy-done.10
  86.5 0.2 copy.34.route_ref
  86.7 0.0 copy-done.11
  86.7 0.0 copy-start.7
  86.7 1.6 copy-done.7
  88.3 103.9 %shard_map.119 = bf16[512,128]{1,0:T(8,128)(2,1)S(1)} custom-call(bf16[512,128]{1,0:T(8,128)(2,1)S(1)} %get-tuple-element.9.mixed_ref, s32[2,512]{1,0:T(2,128)S(1)} %copy.33.slot_row, s32[512,2]{1,0:T(8,128)S(1)} %add.4.slot_col, f32[512,2]{1,0:T(8,128)S(1)} %copy.34.route_ref, f32[16,128]{1,0:T(8,128)S(1)} %bitcast_convert_fusion.gain_ref, ...), custom_call_target="tpu_custom_call" | custom-call | flops 3221225472 | bytes 8388608 | tf_op jit(solution)/shard_map/pallas_call | solution.py:776
  192.2 0.7 copy.36
  (4 shorter events, 0.0 us)
Async XLA Ops:
  2.9 1.0 copy-start
  3.9 1.0 copy-start.1
  5.0 1.0 copy-start.2
  6.0 0.9 copy-start.3
  7.0 0.9 copy-start.4
  7.9 0.7 copy-start.5
  8.6 76.5 %copy-start.9 = (s32[512,2]{0,1:T(2,128)S(1)}, s32[512,2]{0,1:T(2,128)}, u32[]{:S(2)}) copy-start(s32[512,2]{0,1:T(2,128)} %param.19) | copy-start | bytes 12292
  82.4 1.3 copy-start.6
  83.8 1.3 copy-start.8
  85.1 1.4 copy-start.10
  85.1 1.6 copy-start.11
  86.7 1.6 copy-start.7

commit v3 on v1

v3 whole, which is shorter than its diff:
```python
import functools
import math

import jax
import jax.numpy as jnp
from jax import lax
from jax.experimental import pallas as pl
from jax.experimental.pallas import tpu as pltpu
from jax.sharding import PartitionSpec as P

NORM_EPS = 1e-06
CLAMP_LIMIT = 7.0
SILU_ALPHA = 1.702
MESH = pl.DeviceIdType.MESH
GATE_ROWS = 16


def remote(src, dst, send_sem, recv_sem, **where):
    return pltpu.make_async_remote_copy(
        src_ref=src,
        dst_ref=dst,
        send_sem=send_sem,
        recv_sem=recv_sem,
        device_id=where,
        device_id_type=MESH,
    )


def ring_start(n, place, make):
    if n == 4:
        for k in range(2):
            make(place, k, 1, 0, k).start()
            make(place, 1 - k, 3, 1, k).start()
    elif n == 2:
        for k in range(2):
            make(place, k, 1, 0, k).start()


def ring_forward(n, place, make):
    if n == 4:
        before, after = lax.rem(place + 3, 4), lax.rem(place + 1, 4)
        make(before, 0, 1, 0, 2).wait_recv()
        make(before, 0, 1, 0, 2).start()
        make(after, 1, 3, 1, 2).wait_recv()
        make(after, 1, 3, 1, 2).start()


def ring_finish(n, place, make):
    if n == 4:
        make(lax.rem(place + 3, 4), 1, 1, 0, 0).wait_recv()
        make(lax.rem(place + 1, 4), 0, 1, 0, 0).wait_recv()
        for k in range(2):
            make(lax.rem(place + 2, 4), k, 1, 0, 0).wait_recv()
    elif n == 2:
        for k in range(2):
            make(1 - place, k, 1, 0, 0).wait_recv()


def ring_sent(n, place, make):
    if n == 4:
        for k in range(3):
            half = k if k < 2 else 0
            make(place, half, 1, 0, k).wait_send()
            make(place, 1 - half, 3, 1, k).wait_send()
    elif n == 2:
        for k in range(2):
            make(place, k, 1, 0, k).wait_send()


def layer_kernel(
    sp_size,
    tp_size,
    y_size,
    q_ref,
    k_ref,
    v_ref,
    gate_ref,
    residual_ref,
    weight_ref,
    gate_w,
    up_w,
    down_w,
    slot_row,
    slot_col,
    route_ref,
    gain_ref,
    out_ref,
    q_v,
    k_v,
    v_v,
    gate_rows,
    residual_v,
    weight_v,
    mixed_v,
    kv_all,
    qpad,
    wide,
    top,
    total,
    summed,
    att_all,
    outgoing,
    landed,
    tokens,
    normed,
    gate_v,
    up_v,
    down_v,
    hidden,
    produced,
    turned,
    returned,
    in_sem,
    kv_recv,
    own_recv,
    ring_send,
    pair_send,
    att_recv,
    att_send,
    own_w,
    w_recv,
    w_send,
    z_send,
    z_recv,
    t_send,
    t_recv,
    h_send,
    h_recv,
    y_send,
    y_recv,
    r_send,
    r_recv,
):
    chips = sp_size // 2
    ups = chips // 2
    downs = chips - 1 - ups
    sp = lax.axis_index("sp")
    tp = lax.axis_index("tp")
    chip = sp // 2
    core = sp - 2 * chip
    size, rows = q_ref.shape
    half = rows // 2
    x_size = tp_size // y_size
    y = tp // x_size
    x = tp - y * x_size
    quarter = rows // 4
    starts = [0] + [GATE_ROWS + k * quarter for k in range(1, 4)]
    lengths = [GATE_ROWS + quarter] + [quarter] * 3
    parts = range(4)
    up_sp = lax.rem(chip + 1, chips) * 2 + core
    down_sp = lax.rem(chip + chips - 1, chips) * 2 + core
    pair_sp = chip * 2 + 1 - core

    barrier = pltpu.get_barrier_semaphore()
    for d in range(1, sp_size):
        pl.semaphore_signal(
            barrier, inc=1, device_id={"sp": lax.rem(sp + d, sp_size)}, device_id_type=MESH
        )
    for d in range(1, tp_size):
        pl.semaphore_signal(
            barrier, inc=1, device_id={"tp": lax.rem(tp + d, tp_size)}, device_id_type=MESH
        )

    inputs = [
        pltpu.make_async_copy(source, target, in_sem.at[k])
        for k, (source, target) in enumerate(
            (
                (q_ref, q_v),
                (k_ref, k_v),
                (v_ref, v_v),
                (gate_ref, gate_rows),
                (residual_ref, residual_v),
                (weight_ref, weight_v),
            )
        )
    ]
    for load in inputs:
        load.start()
    for load in inputs[:4]:
        load.wait()

    gates = gate_rows[...]
    high = gates.astype(jnp.bfloat16)
    rest = gates - high.astype(jnp.float32)
    middle = rest.astype(jnp.bfloat16)
    low = (rest - middle.astype(jnp.float32)).astype(jnp.bfloat16)
    kv_all[sp, 0:GATE_ROWS, :] = jnp.concatenate(
        [
            high.astype(jnp.float32),
            middle.astype(jnp.float32),
            low.astype(jnp.float32),
            jnp.zeros_like(gates),
        ],
        axis=0,
    ).astype(jnp.bfloat16)
    both_kv = jnp.concatenate([k_v[...], v_v[...]], axis=0).astype(jnp.float32)
    kv_all[sp, GATE_ROWS:, :] = both_kv.T.astype(jnp.bfloat16)
    qs = q_v[...].astype(jnp.float32) * (size**-0.5)
    qpad[...] = jnp.concatenate([qs, jnp.zeros_like(qs)], axis=0).T.astype(jnp.bfloat16)
    first_gate = gates[0:1, 0:1]

    pl.semaphore_wait(barrier, sp_size - 1 + tp_size - 1)

    def piece(slot, part):
        return kv_all.at[slot, pl.ds(starts[part], lengths[part]), :]

    def hop(slot, step, way, part, target):
        return remote(
            piece(slot, part),
            piece(slot, part),
            ring_send.at[step, way, part],
            kv_recv.at[slot, part],
            sp=target,
        )

    def share(slot, step, way):
        return remote(
            kv_all.at[slot],
            kv_all.at[slot],
            pair_send.at[step, way],
            own_recv.at[slot],
            sp=pair_sp,
        )

    matrices = ((gate_w, gate_v), (up_w, up_v), (down_w, down_v))
    depth = gate_w.shape[1]
    columns = weight_ref.shape[1]

    def lanes_of(owner):
        return pl.ds(pl.multiple_of(owner * columns, columns), columns)

    def weight_copy(m):
        own, every = matrices[m]

        def make(owner, k, step, way, index):
            here = every.at[pl.ds(k * (depth // 2), depth // 2), lanes_of(owner)]
            mine = own.at[0, pl.ds(k * (depth // 2), depth // 2), :]
            return remote(
                mine if index < 2 else here,
                here,
                w_send.at[m, way, index],
                w_recv.at[m, owner, k],
                tp=lax.rem(y + step, y_size) * x_size + x,
            )

        return make

    def own_weight(m):
        own, every = matrices[m]
        return pltpu.make_async_copy(own.at[0], every.at[:, lanes_of(y)], own_w.at[m])

    def weight_start(m):
        ring_start(y_size, y, weight_copy(m))
        own_weight(m).start()

    def weight_ready(m):
        ring_finish(y_size, y, weight_copy(m))
        own_weight(m).wait()

    if ups >= 1:
        for part in parts:
            hop(sp, 0, 0, part, up_sp).start()
            if downs >= 1:
                hop(sp, 0, 1, part, down_sp).start()
    share(sp, 0, 0).start()
    for m in range(2):
        weight_start(m)
    for load in inputs[4:]:
        load.wait()

    wide[...] = jnp.zeros_like(wide)
    for h in range(tp_size):
        w = weight_v[h * size : (h + 1) * size, :]
        wide[h * 2 * size : h * 2 * size + size, 0 : w.shape[1]] = w
        wide[h * 2 * size + size : (h + 1) * 2 * size, w.shape[1] :] = w

    top[...] = jnp.full_like(top, -1e30)
    total[...] = jnp.zeros_like(total)
    summed[...] = jnp.zeros_like(summed)
    tile = min(128, rows)
    lanes = 128

    def attend(slot, diagonal):
        parts = kv_all[slot, 0:GATE_ROWS, :].astype(jnp.float32)
        n4 = GATE_ROWS // 4
        key_gates = parts[0:n4] + parts[n4 : 2 * n4] + parts[2 * n4 : 3 * n4]
        shift = first_gate - key_gates
        keys = kv_all[slot, GATE_ROWS:, :]
        for t in range(rows // tile):
            here = slice(t * tile, (t + 1) * tile)
            scores = lax.dot_general(
                qpad[here, :], keys, (((1,), (1,)), ((), ())), preferred_element_type=jnp.float32
            )
            pieces = []
            for j in range(rows // lanes):
                s = scores[:, j * lanes : (j + 1) * lanes] + shift[j : j + 1, :]
                if diagonal:
                    place = lax.broadcasted_iota(jnp.int32, s.shape, 0) + t * tile
                    other = lax.broadcasted_iota(jnp.int32, s.shape, 1) + j * lanes
                    s = jnp.where(other <= place, s, -1e30)
                pieces.append(s)
            most = functools.reduce(jnp.maximum, pieces)
            old = top[here, :]
            new = jnp.maximum(old, jnp.max(most, axis=1, keepdims=True))
            shrink = jnp.exp(old - new)
            raised = [jnp.exp(s - new) for s in pieces]
            total[here, :] = total[here, :] * shrink + functools.reduce(jnp.add, raised)
            weights = jnp.concatenate([r.astype(jnp.bfloat16) for r in raised], axis=1)
            summed[here, :] = summed[here, :] * shrink + jnp.dot(
                weights, keys, preferred_element_type=jnp.float32
            )
            top[here, :] = new

    attend(sp, True)

    def earlier(slot):
        @pl.when(slot < sp)
        def _():
            attend(slot, False)

    def slots(step):
        up_from = lax.rem(chip + chips - step, chips)
        down_from = lax.rem(chip + step, chips)
        return up_from, down_from

    def arrive(slot, step, way, part, target, send):
        hop(slot, step, way, part, target).wait_recv()
        if send is True:
            hop(slot, step, way, part, target).start()
        elif send is not False:

            @pl.when(send)
            def _():
                hop(slot, step, way, part, target).start()

    def partner(step, way, slot):
        share(slot, step, way).wait_recv()
        earlier(slot)

    def both(step):
        up_from, down_from = slots(step)
        before_up, before_down = slots(step - 1)
        up_slot, down_slot = up_from * 2 + core, down_from * 2 + core

        def pieces(these):
            for part in these:
                arrive(up_slot, step, 0, part, up_sp, step < ups)
                arrive(down_slot, step, 1, part, down_sp, step < downs)

        pieces(parts[:2])
        partner(step - 1, 0, before_up * 2 + 1 - core)

        @pl.when(step >= 2)
        def _():
            partner(step - 1, 1, before_down * 2 + 1 - core)

        pieces(parts[2:])
        share(up_slot, step, 0).start()
        share(down_slot, step, 1).start()
        for m in range(2):

            @pl.when(step == max(1, downs - 3 * (1 - m)))
            def _():
                ring_forward(y_size, y, weight_copy(m))

        earlier(up_slot)
        earlier(down_slot)

    if downs >= 1:
        lax.fori_loop(1, downs + 1, lambda i, c: (both(i), c)[1], 0)
    else:
        for m in range(2):
            ring_forward(y_size, y, weight_copy(m))
    last_up, last_down = slots(downs)
    up_from, _ = slots(ups)
    up_slot = up_from * 2 + core
    for part in parts:
        arrive(up_slot, ups, 0, part, up_sp, False)
    share(up_slot, ups, 0).start()
    partner(downs, 0, last_up * 2 + 1 - core)
    if downs >= 1:
        partner(downs, 1, last_down * 2 + 1 - core)
    earlier(up_slot)
    partner(ups, 0, up_from * 2 + 1 - core)

    def finished(lo):
        here = slice(lo, lo + half)
        whole = jnp.sum(total[here, :], axis=1, keepdims=True)
        return summed[here, :] / whole

    left = pltpu.roll(finished(0), size, 1)
    right = finished(half)
    lane = lax.broadcasted_iota(jnp.int32, left.shape, 1)
    att_all[tp] = jnp.where(lane < size, left, right).astype(jnp.bfloat16)

    def give(d):
        return remote(
            att_all.at[tp],
            att_all.at[tp],
            att_send.at[d],
            att_recv.at[tp],
            tp=lax.rem(tp + d, tp_size),
        )

    def take(d):
        owner = lax.rem(tp + tp_size - d, tp_size)
        return remote(
            att_all.at[owner],
            att_all.at[owner],
            att_send.at[d],
            att_recv.at[owner],
            tp=owner,
        )

    for d in range(1, tp_size):
        give(d).start()
    for d in range(1, tp_size):
        take(d).wait_recv()
    weight_start(2)
    projected = jnp.zeros((half, wide.shape[1]), jnp.float32)
    for j in range(tp_size // 2):
        pair = jnp.concatenate([att_all[2 * j], att_all[2 * j + 1]], axis=1)
        projected += jnp.dot(
            pair, wide[j * 4 * size : (j + 1) * 4 * size, :], preferred_element_type=jnp.float32
        )
    for part in range(2):
        here = slice(part * half, (part + 1) * half)
        mixed_v[here, :] = (
            residual_v[here, :].astype(jnp.float32)
            + projected[:, part * columns : (part + 1) * columns]
        ).astype(jnp.bfloat16)


    group = sp_size // y_size
    chunks = 2
    share_rows = 2 * 2 * rows // sp_size // chunks
    height = group * share_rows
    width = tp_size * columns
    hid = y_size * columns
    batch = min(sp_size, max(1, 256 // share_rows))
    span = batch * share_rows

    mixed = mixed_v[...]
    first, second = slot_row[0:1, :], slot_row[1:2, :]

    def near(i):
        j = i // 2
        far = (j + 1) // 2
        odd = j - 2 * (j // 2)
        chip_there = lax.rem(chip + chips + (2 * odd - 1) * far, chips)
        other = i - 2 * j
        return chip_there * 2 + core + other * (1 - 2 * core)

    def send_z(c, i):
        there = near(i)
        return remote(
            outgoing.at[c, there], landed.at[c, sp], z_send.at[c, i], z_recv.at[c, sp], sp=there
        )

    def take_z(c, source):
        return remote(
            outgoing.at[c, sp],
            landed.at[c, source],
            z_send.at[c, 0],
            z_recv.at[c, source],
            sp=source,
        )

    for c in range(chunks):
        for n in range(sp_size // batch):
            start = c * sp_size * share_rows + n * span
            number = lax.broadcasted_iota(jnp.int32, (span, rows), 0) + start
            chosen = jnp.logical_or(number == first, number == second)
            picked = jnp.dot(
                chosen.astype(jnp.float32).astype(jnp.bfloat16),
                mixed,
                preferred_element_type=jnp.float32,
            ).astype(jnp.bfloat16)
            for k in range(batch):
                outgoing[c, n * batch + k] = picked[k * share_rows : (k + 1) * share_rows]
        landed[c, sp] = outgoing[c, sp]
        lax.fori_loop(1, sp_size, lambda i, s: (send_z(c, i).start(), s)[1], 0)

    def give_t(c, i, d, source):
        y_there = source // group
        slot = source - y_there * group
        return remote(
            landed.at[c, source],
            tokens.at[c, slot, tp],
            t_send.at[c, i, d],
            t_recv.at[c],
            tp=y_there * x_size + lax.rem(x + d, x_size),
        )

    def own_t(c, source):
        slot = source - (source // group) * group
        return pltpu.make_async_copy(landed.at[c, source], tokens.at[c, slot, tp], t_recv.at[c])

    def pass_on(c, i, source):
        for d in range(1, x_size):
            give_t(c, i, d, source).start()

        @pl.when(source // group == y)
        def _():
            own_t(c, source).start()

        @pl.when(source // group != y)
        def _():
            give_t(c, i, 0, source).start()

    def arrived(c, i):
        source = near(i)
        take_z(c, source).wait_recv()
        pass_on(c, i, source)

    for c in range(chunks):
        pass_on(c, 0, sp)
        lax.fori_loop(1, sp_size, lambda i, s: (arrived(c, i), s)[1], 0)
        if c == 0:
            ring_forward(y_size, y, weight_copy(2))

    def h_copy(c):
        def make(owner, k, step, way, index):
            here = hidden.at[c, pl.ds(k * (y_size // 2), y_size // 2), owner]
            return remote(
                here,
                here,
                h_send.at[c, way, index],
                h_recv.at[c, owner, k],
                tp=y * x_size + lax.rem(x + step, x_size),
            )

        return make

    for m in range(2):
        weight_ready(m)
    for c in range(chunks):
        pltpu.make_async_copy(tokens.at[c], tokens.at[c], t_recv.at[c]).wait()
        for slot in range(group):
            squares = jnp.zeros((share_rows, columns), jnp.float32)
            for t in range(tp_size):
                piece_t = tokens[c, slot, t].astype(jnp.float32)
                squares += piece_t * piece_t
            scale = lax.rsqrt(jnp.sum(squares, axis=1, keepdims=True) / width + NORM_EPS)
            for t in range(tp_size):
                piece_t = tokens[c, slot, t].astype(jnp.float32)
                normed[
                    slot * share_rows : (slot + 1) * share_rows, t * columns : (t + 1) * columns
                ] = (piece_t * scale * gain_ref[t : t + 1, :]).astype(jnp.bfloat16)
        tile = min(256, hid)
        for n in range(hid // tile):
            cols = slice(n * tile, (n + 1) * tile)
            gate_input = jnp.dot(normed[...], gate_v[:, cols], preferred_element_type=jnp.float32)
            linear_input = jnp.dot(normed[...], up_v[:, cols], preferred_element_type=jnp.float32)
            cut = jnp.minimum(gate_input, CLAMP_LIMIT)
            linear = jnp.clip(linear_input, -CLAMP_LIMIT, CLAMP_LIMIT)
            active = (cut / (1.0 + jnp.exp(-SILU_ALPHA * cut)) * (linear + 1.0)).astype(jnp.bfloat16)
            for k in range(tile // columns):
                hidden[c, n * (tile // columns) + k, x] = active[
                    :, k * columns : (k + 1) * columns
                ]
        ring_start(x_size, x, h_copy(c))

    def give_y(c, d):
        y_there = lax.rem(y + d, y_size)
        return remote(
            produced.at[c, y_there],
            turned.at[c, y],
            y_send.at[c, d],
            y_recv.at[c, y],
            tp=y_there * x_size + x,
        )

    def take_y(c, d):
        source = lax.rem(y + y_size - d, y_size)
        return source, remote(
            produced.at[c, source],
            turned.at[c, source],
            y_send.at[c, d],
            y_recv.at[c, source],
            tp=source * x_size + x,
        )

    def send_r(c, source, slot):
        there = source * group + slot
        return remote(
            turned.at[c, source, pl.ds(slot * share_rows, share_rows), :],
            returned.at[c, sp],
            r_send.at[c, there],
            r_recv.at[c, sp],
            sp=there,
        )

    def give_back(c, source):
        for slot in range(group):
            there = source * group + slot

            @pl.when(there == sp)
            def _():
                returned[c, sp] = turned[
                    c, source, slot * share_rows : (slot + 1) * share_rows, :
                ]

            @pl.when(there != sp)
            def _():
                send_r(c, source, slot).start()

    for c in range(chunks):
        ring_forward(x_size, x, h_copy(c))
    weight_ready(2)
    for c in range(chunks):
        ring_finish(x_size, x, h_copy(c))
        made = jnp.zeros((height, hid), jnp.float32)
        for t in range(0, tp_size, 2):
            k, j = t // x_size, t % x_size
            pair = jnp.concatenate([hidden[c, k, j], hidden[c, k, j + 1]], axis=1)
            made += jnp.dot(
                pair,
                down_v[t * columns : (t + 2) * columns, :],
                preferred_element_type=jnp.float32,
            )
        for k in range(y_size):
            produced[c, k] = made[:, k * columns : (k + 1) * columns].astype(jnp.bfloat16)
        for d in range(1, y_size):
            give_y(c, d).start()
        turned[c, y] = produced[c, y]
        give_back(c, y)
    for c in range(chunks):
        for d in range(1, y_size):
            source, copy = take_y(c, d)
            copy.wait_recv()
            give_back(c, source)

    sums = [jnp.zeros((rows, columns), jnp.float32) for _ in range(2)]
    for c in range(chunks):
        for n in range(sp_size // batch):
            for k in range(batch):
                e = n * batch + k

                @pl.when(sp != e)
                def _():
                    remote(
                        turned.at[c, 0, pl.ds(0, share_rows), :],
                        returned.at[c, e],
                        r_send.at[c, e],
                        r_recv.at[c, e],
                        sp=sp,
                    ).wait_recv()

            block = jnp.concatenate([returned[c, n * batch + k] for k in range(batch)], axis=0)
            start = c * sp_size * share_rows + n * span
            number = lax.broadcasted_iota(jnp.int32, (rows, span), 1) + start
            for k in range(2):
                chosen = (number == slot_col[:, k : k + 1]).astype(jnp.float32).astype(jnp.bfloat16)
                sums[k] += jnp.dot(chosen, block, preferred_element_type=jnp.float32)
    blended = route_ref[:, 0:1] * sums[0] + route_ref[:, 1:2] * sums[1]
    out_ref[...] = (mixed.astype(jnp.float32) + blended).astype(jnp.bfloat16)

    if ups >= 1:
        for step in range(ups):
            for part in parts:
                hop(sp, step, 0, part, up_sp).wait_send()
        for step in range(downs):
            for part in parts:
                hop(sp, step, 1, part, down_sp).wait_send()
        for step in range(1, ups + 1):
            share(sp, step, 0).wait_send()
        for step in range(1, downs + 1):
            share(sp, step, 1).wait_send()
    share(sp, 0, 0).wait_send()
    for d in range(1, tp_size):
        give(d).wait_send()


    for m in range(3):
        ring_sent(y_size, y, weight_copy(m))
    for c in range(chunks):
        for i in range(1, sp_size):
            send_z(c, i).wait_send()
        for i in range(sp_size):
            for d in range(1, x_size):
                give_t(c, i, d, sp).wait_send()

            @pl.when(near(i) // group != y)
            def _():
                give_t(c, i, 0, sp).wait_send()

        ring_sent(x_size, x, h_copy(c))
        for d in range(1, y_size):
            give_y(c, d).wait_send()
        for e in range(sp_size):

            @pl.when(sp != e)
            def _():
                send_r(c, e // group, e % group).wait_send()


def y_of(tp_size):
    return math.isqrt(tp_size)


def layer(
    mesh,
    query_rows,
    key_rows,
    value_rows,
    cum_gates,
    residual,
    output_weight,
    norm_gain,
    slot,
    route_weights,
    gate_weight,
    up_weight,
    down_weight,
):
    sp_size, tp_size = mesh.shape["sp"], mesh.shape["tp"]
    y_size = y_of(tp_size)
    x_size = tp_size // y_size
    rows, size = query_rows.shape
    columns = output_weight.shape[1]
    group = sp_size // y_size
    depth = gate_weight.shape[1]
    hid = y_size * columns
    part = 2 * rows // sp_size
    height = group * part
    steps = sp_size // 4 + 1
    bf16, f32 = jnp.bfloat16, jnp.float32
    vmem = pl.BlockSpec(memory_space=pltpu.VMEM)
    anywhere = pl.BlockSpec(memory_space=pl.ANY)
    dma = pltpu.SemaphoreType.DMA
    gates = cum_gates.reshape(4, rows // 4)
    return pl.pallas_call(
        functools.partial(layer_kernel, sp_size, tp_size, y_size),
        out_shape=jax.ShapeDtypeStruct((rows, columns), bf16),
        in_specs=[anywhere] * 9 + [vmem] * 4,
        out_specs=vmem,
        scratch_shapes=[
            pltpu.VMEM((size, rows), bf16),
            pltpu.VMEM((size, rows), bf16),
            pltpu.VMEM((size, rows), bf16),
            pltpu.VMEM(gates.shape, f32),
            pltpu.VMEM(residual.shape, bf16),
            pltpu.VMEM(output_weight.shape, bf16),
            pltpu.VMEM((rows, columns), bf16),
            pltpu.VMEM((sp_size, GATE_ROWS + rows, 2 * size), bf16),
            pltpu.VMEM((rows, 2 * size), bf16),
            pltpu.VMEM((tp_size * 2 * size, 2 * columns), bf16),
            pltpu.VMEM((rows, 2 * size), f32),
            pltpu.VMEM((rows, 2 * size), f32),
            pltpu.VMEM((rows, 2 * size), f32),
            pltpu.VMEM((tp_size, rows // 2, 2 * size), bf16),
            pltpu.VMEM((2, sp_size, part, columns), bf16),
            pltpu.VMEM((2, sp_size, part, columns), bf16),
            pltpu.VMEM((2, group, tp_size, part, columns), bf16),
            pltpu.VMEM((height, tp_size * columns), bf16),
            pltpu.VMEM((depth, hid), bf16),
            pltpu.VMEM((depth, hid), bf16),
            pltpu.VMEM((depth, hid), bf16),
            pltpu.VMEM((2, y_size, x_size, height, columns), bf16),
            pltpu.VMEM((2, y_size, height, columns), bf16),
            pltpu.VMEM((2, y_size, height, columns), bf16),
            pltpu.VMEM((2, sp_size, part, columns), bf16),
            dma((6,)),
            dma((sp_size, 4)),
            dma((sp_size,)),
            dma((steps, 2, 4)),
            dma((steps, 2)),
            dma((tp_size,)),
            dma((tp_size,)),
            dma((3,)),
            dma((3, y_size, 2)),
            dma((3, 2, 3)),
            dma((2, sp_size)),
            dma((2, sp_size)),
            dma((2, sp_size, x_size)),
            dma((2,)),
            dma((2, 2, 3)),
            dma((2, x_size, 2)),
            dma((2, y_size)),
            dma((2, y_size)),
            dma((2, sp_size)),
            dma((2, sp_size)),
        ],
        compiler_params=pltpu.CompilerParams(
            collective_id=0, has_side_effects=True, vmem_limit_bytes=60 << 20
        ),
    )(
        query_rows.T,
        key_rows.T,
        value_rows.T,
        gates,
        residual,
        output_weight,
        gate_weight,
        up_weight,
        down_weight,
        slot.T,
        slot,
        route_weights,
        norm_gain.astype(f32).reshape(tp_size, columns),
    )


def slots_of(expert_index, count):
    rows, topk = expert_index.shape
    chosen = expert_index.reshape(rows * topk)
    matches = chosen[:, None] == jnp.arange(count, dtype=jnp.int32)[None, :]
    order = jnp.arange(rows * topk, dtype=jnp.int32)
    before = (order[None, :] < order[:, None]).astype(jnp.bfloat16)
    ahead = jnp.dot(before, matches.astype(jnp.bfloat16), preferred_element_type=jnp.float32)
    rank = jnp.sum(jnp.where(matches, ahead, 0.0), axis=1).astype(jnp.int32)
    part = rows * topk // count
    half = rank // part
    return (half * count * part + chosen * part + rank - half * part).reshape(rows, topk)


def body(
    mesh,
    query_rows,
    key_rows,
    value_rows,
    cum_gates,
    residual,
    output_weight,
    norm_gain,
    expert_index,
    route_weights,
    gate_weight,
    up_weight,
    down_weight,
):
    slot = slots_of(expert_index, mesh.shape["sp"])
    return layer(
        mesh,
        query_rows,
        key_rows,
        value_rows,
        cum_gates,
        residual,
        output_weight,
        norm_gain,
        slot,
        route_weights,
        gate_weight,
        up_weight,
        down_weight,
    )


def solution(mesh):
    placed = (
        P("sp", "tp"),
        P("sp", "tp"),
        P("sp", "tp"),
        P("sp", "tp"),
        P("sp", "tp"),
        P(None, "tp"),
        P(),
        P("sp", None),
        P("sp", None),
        P("sp", None, "tp"),
        P("sp", None, "tp"),
        P("sp", None, "tp"),
    )
    return jax.shard_map(
        functools.partial(body, mesh),
        mesh=mesh,
        in_specs=placed,
        out_specs=P("sp", "tp"),
        check_vma=False,
    )
```

time: 401 us -> 179 us (0.45)
  the two profiles are of different devices: /device:TPU:25 before, /device:TPU:17 now
where the time goes in v3:
time: 179 us
  Pallas kernels  172 us (96%)
  local copies, waits for them, and re-layouts  4.78 us (3%)
    pallas_call x1, Pallas kernels, layer(): pl.pallas_call(functools.partial(layer_kernel, sp_size, tp_size, y_size),...  172 us

profile of v3, /device:TPU:17, one launch (start us, length us, event | category | flops | bytes accessed | tf_op | source)
XLA Modules:
  0.0 178.6 jit_solution(6107538967593875578)
XLA Ops:
  0.0 0.8 copy.26
  0.8 0.2 eq.15
  1.0 0.5 fusion.2
  1.6 0.0 copy-start.1
  1.6 0.2 convert_element_type.11
  1.8 0.1 add_select_fusion
  1.9 0.1 copy.27
  2.0 0.2 copy-done.1
  2.3 0.1 copy.29
  2.4 0.0 copy-start.2
  2.4 0.0 copy-start.3
  2.4 0.2 multiply_subtract_fusion.slot_col
  2.6 0.0 copy-start
  2.6 0.7 copy.30.slot_row
  3.3 0.0 copy-done.2
  3.3 0.8 copy.31.route_ref
  4.2 0.0 copy-done.3
  4.2 0.6 bitcast_convert_fusion.gain_ref
  4.8 0.0 copy-done
  4.8 172.3 %shard_map.118 = bf16[512,128]{1,0:T(8,128)(2,1)} custom-call(bf16[64,512]{1,0:T(8,128)(2,1)} %bitcast.9, bf16[64,512]{1,0:T(8,128)(2,1)} %bitcast.10, bf16[64,512]{1,0:T(8,128)(2,1)} %bitcast.11, f32[4,128]{1,0:T(4,128)} %bitcast.12, bf16[512,128]{1,0:T(8,128)(2,1)} %residual_ref.1, bf16[1024,128]{1,0:T(8,128)(2,1)} %weight_ref.1, ...), custom_call_target="tpu_custom_call" | custom-call | tf_op jit(solution)/shard_map/pallas_call | solution.py:733
  177.1 1.6 copy.33
  (2 shorter events, 0.0 us)
Async XLA Ops:
  1.6 0.7 copy-start.1
  2.4 0.9 copy-start.2
  2.4 1.8 copy-start.3
  2.6 2.2 %copy-start = (s32[512,2]{1,0:T(8,128)}, s32[512,2]{1,0:T(8,128)S(1)}, u32[]{:S(2)}) copy-start(s32[512,2]{1,0:T(8,128)S(1)} %multiply_subtract_fusion.slot_col) | copy-start | bytes 12292

commit v4 on v3

--- a/solution.py
+++ b/solution.py
@@ -152,10 +152,8 @@
     pair_sp = chip * 2 + 1 - core
 
     barrier = pltpu.get_barrier_semaphore()
-    for d in range(1, sp_size):
-        pl.semaphore_signal(
-            barrier, inc=1, device_id={"sp": lax.rem(sp + d, sp_size)}, device_id_type=MESH
-        )
+    for target in (up_sp, down_sp, pair_sp):
+        pl.semaphore_signal(barrier, inc=1, device_id={"sp": target}, device_id_type=MESH)
     for d in range(1, tp_size):
         pl.semaphore_signal(
             barrier, inc=1, device_id={"tp": lax.rem(tp + d, tp_size)}, device_id_type=MESH
@@ -199,7 +197,7 @@
     qpad[...] = jnp.concatenate([qs, jnp.zeros_like(qs)], axis=0).T.astype(jnp.bfloat16)
     first_gate = gates[0:1, 0:1]
 
-    pl.semaphore_wait(barrier, sp_size - 1 + tp_size - 1)
+    pl.semaphore_wait(barrier, 3 + tp_size - 1)
 
     def piece(slot, part):
         return kv_all.at[slot, pl.ds(starts[part], lengths[part]), :]
@@ -277,7 +275,7 @@
     top[...] = jnp.full_like(top, -1e30)
     total[...] = jnp.zeros_like(total)
     summed[...] = jnp.zeros_like(summed)
-    tile = min(128, rows)
+    tile = rows
     lanes = 128
 
     def attend(slot, diagonal):
@@ -513,12 +511,6 @@
         take_z(c, source).wait_recv()
         pass_on(c, i, source)
 
-    for c in range(chunks):
-        pass_on(c, 0, sp)
-        lax.fori_loop(1, sp_size, lambda i, s: (arrived(c, i), s)[1], 0)
-        if c == 0:
-            ring_forward(y_size, y, weight_copy(2))
-
     def h_copy(c):
         def make(owner, k, step, way, index):
             here = hidden.at[c, pl.ds(k * (y_size // 2), y_size // 2), owner]
@@ -532,9 +524,7 @@
 
         return make
 
-    for m in range(2):
-        weight_ready(m)
-    for c in range(chunks):
+    def produce(c):
         pltpu.make_async_copy(tokens.at[c], tokens.at[c], t_recv.at[c]).wait()
         for slot in range(group):
             squares = jnp.zeros((share_rows, columns), jnp.float32)
@@ -560,6 +550,22 @@
                     :, k * columns : (k + 1) * columns
                 ]
         ring_start(x_size, x, h_copy(c))
+
+
+    def arrivals(c, low, high):
+        lax.fori_loop(low, high, lambda i, s: (arrived(c, i), s)[1], 0)
+
+    middle = sp_size // 2
+    pass_on(0, 0, sp)
+    arrivals(0, 1, sp_size)
+    ring_forward(y_size, y, weight_copy(2))
+    pass_on(1, 0, sp)
+    arrivals(1, 1, middle)
+    for m in range(2):
+        weight_ready(m)
+    produce(0)
+    arrivals(1, middle, sp_size)
+    produce(1)
 
     def give_y(c, d):
         y_there = lax.rem(y + d, y_size)

time: 179 us -> 163 us (0.911)
  the two profiles are of different devices: /device:TPU:17 before, /device:TPU:25 now
where the time goes in v4:
time: 163 us; the launch traced here: 161 us
  Pallas kernels  155 us (95%)
  local copies, waits for them, and re-layouts  4.78 us (3%)
    pallas_call x1, Pallas kernels, layer(): pl.pallas_call(functools.partial(layer_kernel, sp_size, tp_size, y_size),...  155 us
    unnamed x11, local copies, waits for them, and re-layouts  3.47 us

profile of v4, /device:TPU:25, one launch (start us, length us, event | category | flops | bytes accessed | tf_op | source)
XLA Modules:
  0.0 161.1 jit_solution(11670401758857588676)
XLA Ops:
  0.0 0.8 copy.26
  0.8 0.2 eq.15
  1.0 0.5 fusion.2
  1.6 0.0 copy-start.1
  1.6 0.2 convert_element_type.11
  1.8 0.1 add_select_fusion
  1.9 0.1 copy.27
  2.0 0.2 copy-done.1
  2.3 0.1 copy.29
  2.4 0.0 copy-start.2
  2.4 0.0 copy-start.3
  2.4 0.2 multiply_subtract_fusion.slot_col
  2.6 0.0 copy-start
  2.6 0.7 copy.30.slot_row
  3.3 0.0 copy-done.2
  3.3 0.8 copy.31.route_ref
  4.2 0.0 copy-done.3
  4.2 0.6 bitcast_convert_fusion.gain_ref
  4.8 0.0 copy-done
  4.8 154.8 %shard_map.118 = bf16[512,128]{1,0:T(8,128)(2,1)} custom-call(bf16[64,512]{1,0:T(8,128)(2,1)} %bitcast.9, bf16[64,512]{1,0:T(8,128)(2,1)} %bitcast.10, bf16[64,512]{1,0:T(8,128)(2,1)} %bitcast.11, f32[4,128]{1,0:T(4,128)} %bitcast.12, bf16[512,128]{1,0:T(8,128)(2,1)} %residual_ref.1, bf16[1024,128]{1,0:T(8,128)(2,1)} %weight_ref.1, ...), custom_call_target="tpu_custom_call" | custom-call | tf_op jit(solution)/shard_map/pallas_call | solution.py:739
  159.6 1.6 copy.33
  (2 shorter events, 0.0 us)
Async XLA Ops:
  1.6 0.7 copy-start.1
  2.4 0.9 copy-start.2
  2.4 1.8 %copy-start.3 = (bf16[2048]{0:T(1024)(128)(2,1)S(1)}, bf16[2048]{0:T(1024)(128)(2,1)}, u32[]{:S(2)}) copy-start(bf16[2048]{0:T(1024)(128)(2,1)} %param.18) | copy-start | bytes 12292
  2.6 2.2 %copy-start = (s32[512,2]{1,0:T(8,128)}, s32[512,2]{1,0:T(8,128)S(1)}, u32[]{:S(2)}) copy-start(s32[512,2]{1,0:T(8,128)S(1)} %multiply_subtract_fusion.slot_col) | copy-start | bytes 12292

commit v5 on v4

--- a/solution.py
+++ b/solution.py
@@ -477,7 +477,7 @@
             for k in range(batch):
                 outgoing[c, n * batch + k] = picked[k * share_rows : (k + 1) * share_rows]
         landed[c, sp] = outgoing[c, sp]
-        lax.fori_loop(1, sp_size, lambda i, s: (send_z(c, i).start(), s)[1], 0)
+        lax.fori_loop(1, sp_size, lambda i, s: (send_z(c, sp_size - i).start(), s)[1], 0)
 
     def give_t(c, i, d, source):
         y_there = source // group
@@ -553,7 +553,7 @@
 
 
     def arrivals(c, low, high):
-        lax.fori_loop(low, high, lambda i, s: (arrived(c, i), s)[1], 0)
+        lax.fori_loop(low, high, lambda i, s: (arrived(c, sp_size - i), s)[1], 0)
 
     middle = sp_size // 2
     pass_on(0, 0, sp)
@@ -587,10 +587,13 @@
             tp=source * x_size + x,
         )
 
+    def row_of(slot):
+        return pl.multiple_of(slot * share_rows, share_rows)
+
     def send_r(c, source, slot):
         there = source * group + slot
         return remote(
-            turned.at[c, source, pl.ds(slot * share_rows, share_rows), :],
+            turned.at[c, source, pl.ds(row_of(slot), share_rows), :],
             returned.at[c, sp],
             r_send.at[c, there],
             r_recv.at[c, sp],
@@ -598,13 +601,14 @@
         )
 
     def give_back(c, source):
-        for slot in range(group):
+        for k in range(group):
+            slot = lax.rem(sp + k, group)
             there = source * group + slot
 
             @pl.when(there == sp)
             def _():
                 returned[c, sp] = turned[
-                    c, source, slot * share_rows : (slot + 1) * share_rows, :
+                    c, source, pl.ds(row_of(slot), share_rows), :
                 ]
 
             @pl.when(there != sp)

time: 163 us -> 166 us (1.018)
  the two profiles are of different devices: /device:TPU:25 before, /device:TPU:9 now
where the time goes in v5:
time: 166 us
  Pallas kernels  160 us (96%)
  local copies, waits for them, and re-layouts  4.78 us (3%)
    pallas_call x1, Pallas kernels, layer(): pl.pallas_call(functools.partial(layer_kernel, sp_size, tp_size, y_size),...  160 us
    unnamed x11, local copies, waits for them, and re-layouts  3.47 us

profile of v5, /device:TPU:9, one launch (start us, length us, event | category | flops | bytes accessed | tf_op | source)
XLA Modules:
  0.0 166.2 jit_solution(18434946284759665739)
XLA Ops:
  0.0 0.8 copy.26
  0.8 0.2 eq.15
  1.0 0.5 fusion.2
  1.6 0.0 copy-start.1
  1.6 0.2 convert_element_type.11
  1.8 0.1 add_select_fusion
  1.9 0.1 copy.27
  2.0 0.2 copy-done.1
  2.3 0.1 copy.29
  2.4 0.0 copy-start.2
  2.4 0.0 copy-start.3
  2.4 0.2 multiply_subtract_fusion.slot_col
  2.6 0.0 copy-start
  2.6 0.7 copy.30.slot_row
  3.3 0.0 copy-done.2
  3.3 0.8 copy.31.route_ref
  4.2 0.0 copy-done.3
  4.2 0.6 bitcast_convert_fusion.gain_ref
  4.8 0.0 copy-done
  4.8 159.8 %shard_map.118 = bf16[512,128]{1,0:T(8,128)(2,1)} custom-call(bf16[64,512]{1,0:T(8,128)(2,1)} %bitcast.9, bf16[64,512]{1,0:T(8,128)(2,1)} %bitcast.10, bf16[64,512]{1,0:T(8,128)(2,1)} %bitcast.11, f32[4,128]{1,0:T(4,128)} %bitcast.12, bf16[512,128]{1,0:T(8,128)(2,1)} %residual_ref.1, bf16[1024,128]{1,0:T(8,128)(2,1)} %weight_ref.1, ...), custom_call_target="tpu_custom_call" | custom-call | tf_op jit(solution)/shard_map/pallas_call | solution.py:743
  164.6 1.6 copy.33
  (2 shorter events, 0.0 us)
Async XLA Ops:
  1.6 0.7 copy-start.1
  2.4 0.9 copy-start.2
  2.4 1.8 %copy-start.3 = (bf16[2048]{0:T(1024)(128)(2,1)S(1)}, bf16[2048]{0:T(1024)(128)(2,1)}, u32[]{:S(2)}) copy-start(bf16[2048]{0:T(1024)(128)(2,1)} %param.18) | copy-start | bytes 12292
  2.6 2.2 %copy-start = (s32[512,2]{1,0:T(8,128)}, s32[512,2]{1,0:T(8,128)S(1)}, u32[]{:S(2)}) copy-start(s32[512,2]{1,0:T(8,128)S(1)} %multiply_subtract_fusion.slot_col) | copy-start | bytes 12292
